TPU v7x, 32 devices: a whole 2x2x4 slice. The times are simulated.
32 devices in a mesh: sp: 16 (over z, y, core), tp: 2 (over x).
Axes of the slice: x: 2, y: 2, z: 4, core: 2. Of those that a mesh axis runs over, the one named last changes fastest.
Arguments:
- inputs: bfloat16 [8192, 3072], P('sp', 'tp'), may hold values from -6 to 6
- w_query: bfloat16 [3072, 1536], P(None, 'tp'), may hold values from -0.109375 to 0.109375
- w_key: bfloat16 [3072, 1536], P(None, 'tp'), may hold values from -0.109375 to 0.109375
- w_value: bfloat16 [3072, 1536], P(None, 'tp'), may hold values from -0.109375 to 0.109375
- rel_bias: float32 [320, 24], P(None, 'tp'), may hold values from -5 to 254
- d_out: bfloat16 [8192, 1536], P('sp', 'tp'), may hold values from -6 to 6
Outputs:
- grad_inputs: bfloat16 [8192, 3072], P('sp', 'tp')
- grad_w_query: float32 [3072, 1536], P('sp', 'tp')
- grad_w_key: float32 [3072, 1536], P('sp', 'tp')
- grad_w_value: float32 [3072, 1536], P('sp', 'tp')
- grad_bias: float32 [320, 24], P(None, 'tp')
All inputs are finite; a program needn't handle non-finite values.
Results may differ from a plain program's by a relative error of at most 0.015.
Values may be sent and summed in bfloat16 or wider, within the bound.
A program may use at most 128 MiB of HBM per device.

v0:
```python
import functools

import jax
import jax.numpy as jnp
import numpy as np
from jax import lax
from jax.experimental import pallas as pl
from jax.experimental.pallas import tpu as pltpu
from jax.sharding import PartitionSpec as P

HEAD = 64
SEG = 64
LEFT = 4
REL_MAX = 256
LANES = 128
QB = 2 * SEG
HALO = LEFT * SEG
KB = HALO + QB
LINE = 512
UNSEEN = -1e30


def passed_along(block, axis, distance):
    devices = range(lax.axis_size(axis))
    route = [(i - distance, i) for i in devices if i - distance in devices]
    return lax.ppermute(block, axis, route)


def dot32(a, b, dims):
    return lax.dot_general(a, b, (dims, ((), ())), preferred_element_type=jnp.float32)


def attention_body(
    line_ref, keep_ref, flip_ref, q_ref, pk_ref, k_ref, pv_ref, v_ref, d_ref,
    dq_ref, dkh_ref, dk_ref, dvh_ref, dv_ref, dline_ref,
    bias, bias_sum, k_ext, v_ext, dk_ext, dv_ext,
):
    blocks = q_ref.shape[0] // QB
    key_row = lax.broadcasted_iota(jnp.int32, (KB, QB), 0)
    query_row = lax.broadcasted_iota(jnp.int32, (KB, QB), 1)
    offset = key_row - jnp.where(query_row < SEG, 0, SEG)
    seen = (offset >= 0) & (offset < HALO + SEG)
    for half in range(2):
        line = jnp.broadcast_to(line_ref[0, half : half + 1, :], (KB, LINE))
        skewed = pltpu.roll(line, 0, 1, stride=1, stride_axis=0)[:, :QB]
        bias[:, half * QB : (half + 1) * QB] = jnp.where(seen, skewed, UNSEEN)
    k_ext[:HALO, :] = pk_ref[...]
    k_ext[HALO:, :] = k_ref[...]
    v_ext[:HALO, :] = pv_ref[...]
    v_ext[HALO:, :] = v_ref[...]
    dk_ext[...] = jnp.zeros_like(dk_ext)
    dv_ext[...] = jnp.zeros_like(dv_ext)
    bias_sum[...] = jnp.zeros_like(bias_sum)
    lane = lax.broadcasted_iota(jnp.int32, (QB, LANES), 1)
    scale = HEAD ** (-0.5)
    zero = jnp.zeros((QB, LANES), jnp.bfloat16)

    def stacked(rows):
        return jnp.concatenate(
            [jnp.where(lane < HEAD, rows, zero), jnp.where(lane < HEAD, zero, rows)], axis=0
        )

    for block in range(blocks):
        keys = slice(block * QB, block * QB + KB)
        rows = slice(block * QB, (block + 1) * QB)
        q2 = stacked(q_ref[rows, :] * jnp.bfloat16(scale))
        d2 = stacked(d_ref[rows, :])
        k = k_ext[keys, :]
        v = v_ext[keys, :]
        score = dot32(k, q2, ((1,), (1,))) + bias[...]
        if block * QB < HALO:
            score = score + keep_ref[keys, :]
        top = jnp.max(score, axis=0, keepdims=True)
        power = jnp.exp(score - top)
        prob = power * (1.0 / jnp.sum(power, axis=0, keepdims=True))
        prob_low = prob.astype(jnp.bfloat16)
        grad_prob = dot32(v, d2, ((1,), (1,)))
        delta = jnp.sum(prob_low.astype(jnp.float32) * grad_prob, axis=0, keepdims=True)
        dscore = prob * (grad_prob - delta)
        bias_sum[...] += dscore
        dscore_low = dscore.astype(jnp.bfloat16)
        dv_ext[keys, :] += dot32(prob_low, d2, ((1,), (0,)))
        dk_ext[keys, :] += dot32(dscore_low, q2, ((1,), (0,)))
        dq_t = dot32(k, dscore_low, ((0,), (0,)))
        dq_t = jnp.concatenate([dq_t[:HEAD, :QB], dq_t[HEAD:, QB:]], axis=0)
        dq_ref[rows, :] = (dq_t.T * scale).astype(jnp.bfloat16)

    dkh_ref[...] = dk_ext[:HALO, :].astype(jnp.bfloat16)
    dk_ref[...] = dk_ext[HALO:, :]
    dvh_ref[...] = dv_ext[:HALO, :].astype(jnp.bfloat16)
    dv_ref[...] = dv_ext[HALO:, :]
    flipped = lax.dot_general(
        flip_ref[...], bias_sum[...], (((1,), (0,)), ((), ())),
        precision=lax.Precision.HIGHEST, preferred_element_type=jnp.float32,
    )
    for half in range(2):
        part = flipped[:, half * QB : (half + 1) * QB]
        wide = jnp.concatenate([part, jnp.zeros((KB, LINE - QB), jnp.float32)], axis=1)
        skewed = pltpu.roll(wide, 0, 1, stride=1, stride_axis=0)
        dline_ref[0, half : half + 1, :] = jnp.sum(skewed, axis=0, keepdims=True)


def attention(lines, keep, flip, query, prior_key, key, prior_value, value, d_out):
    tok_rows, width = query.shape
    pairs = width // LANES
    ext = HALO + tok_rows

    def column(rows):
        return pl.BlockSpec((rows, LANES), lambda i: (0, i))

    def fixed(shape):
        return pl.BlockSpec(shape, lambda i: (0,) * len(shape))

    line_spec = pl.BlockSpec((1, 2, LINE), lambda i: (i, 0, 0))
    sds = jax.ShapeDtypeStruct
    elements = pairs * (tok_rows // QB) * KB * 2 * QB
    return pl.pallas_call(
        attention_body,
        grid=(pairs,),
        in_specs=[
            line_spec, fixed(keep.shape), fixed(flip.shape), column(tok_rows), column(HALO),
            column(tok_rows), column(HALO), column(tok_rows), column(tok_rows),
        ],
        out_specs=[
            column(tok_rows), column(HALO), column(tok_rows), column(HALO), column(tok_rows),
            line_spec,
        ],
        out_shape=[
            sds((tok_rows, width), jnp.bfloat16),
            sds((HALO, width), jnp.bfloat16),
            sds((tok_rows, width), jnp.float32),
            sds((HALO, width), jnp.bfloat16),
            sds((tok_rows, width), jnp.float32),
            sds((pairs, 2, LINE), jnp.float32),
        ],
        scratch_shapes=[
            pltpu.VMEM((KB, 2 * QB), jnp.float32),
            pltpu.VMEM((KB, 2 * QB), jnp.float32),
            pltpu.VMEM((ext, LANES), jnp.bfloat16),
            pltpu.VMEM((ext, LANES), jnp.bfloat16),
            pltpu.VMEM((ext, LANES), jnp.float32),
            pltpu.VMEM((ext, LANES), jnp.float32),
        ],
        cost_estimate=pl.CostEstimate(
            flops=elements * LANES * 10, bytes_accessed=tok_rows * width * 20,
            transcendentals=elements,
        ),
        name="attention",
    )(lines, keep, flip, query, prior_key, key, prior_value, value, d_out)


def weight_body(x_ref, *refs):
    out_ref = refs[-1]
    width = refs[0].shape[1]
    for at, grad_ref in enumerate(refs[:-1]):
        part = dot32(x_ref[...], grad_ref[...], ((0,), (0,)))
        out_ref[:, at * width : (at + 1) * width] = part.astype(out_ref.dtype)


def weight_product(whole, grads):
    rows, features = whole.shape
    width = grads[0].shape[1]
    total = width * len(grads)
    tile = 512
    return pl.pallas_call(
        weight_body,
        grid=(features // tile,),
        in_specs=[pl.BlockSpec((rows, tile), lambda i: (0, i))]
        + [pl.BlockSpec((rows, width), lambda i: (0, 0))] * len(grads),
        out_specs=pl.BlockSpec((tile, total), lambda i: (i, 0)),
        out_shape=jax.ShapeDtypeStruct((features, total), jnp.bfloat16),
        cost_estimate=pl.CostEstimate(
            flops=2 * rows * features * total,
            bytes_accessed=2 * (rows * features + rows * total + features * total),
            transcendentals=0,
        ),
        name="weight_product",
    )(whole, *grads)


def summed(block, axis):
    size = lax.axis_size(axis)
    if size & (size - 1):
        return lax.psum(block, axis)
    step = 1
    while step < size:
        block = block + lax.ppermute(block, axis, [(i, i ^ step) for i in range(size)])
        step *= 2
    return block


def scattered(partial, axis):
    size = lax.axis_size(axis)
    me = lax.axis_index(axis)
    width = partial.shape[1] // size
    total = lax.dynamic_slice_in_dim(partial, me * width, width, 1).astype(jnp.float32)
    for step in range(1, size):
        away = lax.dynamic_slice_in_dim(partial, ((me + step) % size) * width, width, 1)
        got = lax.ppermute(away, axis, [(i, (i + step) % size) for i in range(size)])
        total = total + got.astype(jnp.float32)
    return total.astype(partial.dtype)


def local(inputs, w_query, w_key, w_value, rel_bias, d_out):
    tok_rows = inputs.shape[0]
    width = d_out.shape[1]
    pairs = width // LANES
    first_row = lax.axis_index("sp") * tok_rows
    whole = lax.all_gather(inputs, "tp", axis=1, tiled=True)

    place = np.arange(LINE)
    apart = np.where(place < QB, place, place - LINE)
    table_rows = np.arange(rel_bias.shape[0])
    index = np.clip(HALO + apart, 1 - SEG, REL_MAX) + SEG - 1
    onehot = (index[:, None] == table_rows[None, :]).astype(np.float32)
    lines = lax.dot_general(
        rel_bias, jnp.asarray(onehot), (((0,), (1,)), ((), ())),
        precision=lax.Precision.HIGHEST, preferred_element_type=jnp.float32,
    ).reshape(pairs, 2, LINE)
    key_pos = first_row - HALO + jnp.arange(KB + HALO)
    keep = jnp.broadcast_to(
        jnp.where(key_pos >= 0, 0.0, UNSEEN).astype(jnp.float32)[:, None], (KB + HALO, 2 * QB)
    )
    flip = jnp.asarray(np.eye(KB, dtype=np.float32)[::-1].copy())

    key = dot32(whole, w_key, ((1,), (0,))).astype(jnp.bfloat16)
    prior_key = passed_along(key[tok_rows - HALO :], "sp", 1)
    value = dot32(whole, w_value, ((1,), (0,))).astype(jnp.bfloat16)
    prior_value = passed_along(value[tok_rows - HALO :], "sp", 1)
    query = dot32(whole, w_query, ((1,), (0,))).astype(jnp.bfloat16)
    grad_query, key_halo, key_own, value_halo, value_own, dlines = attention(
        lines, keep, flip, query, prior_key, key, prior_value, value, d_out
    )
    back_key = passed_along(key_halo, "sp", -1)
    back_value = passed_along(value_halo, "sp", -1)

    def joined(own, back):
        late = own[tok_rows - HALO :] + back.astype(jnp.float32)
        return jnp.concatenate([own[: tok_rows - HALO], late], axis=0).astype(jnp.bfloat16)

    grad_key = joined(key_own, back_key)
    grad_value = joined(value_own, back_value)

    weight_grads = lax.psum_scatter(
        weight_product(whole, (grad_query, grad_key, grad_value)),
        "sp", scatter_dimension=0, tiled=True,
    ).astype(jnp.float32)
    grad_w_query = weight_grads[:, :width]
    grad_w_key = weight_grads[:, width : 2 * width]
    grad_w_value = weight_grads[:, 2 * width :]

    diagonal = np.arange(LINE) - (KB - 1)
    back_index = np.clip(HALO + diagonal, 1 - SEG, REL_MAX) + SEG - 1
    back_onehot = (table_rows[:, None] == back_index[None, :]).astype(np.float32)
    local_bias = lax.dot_general(
        jnp.asarray(back_onehot), dlines.reshape(2 * pairs, LINE), (((1,), (1,)), ((), ())),
        precision=lax.Precision.HIGHEST, preferred_element_type=jnp.float32,
    )
    grad_bias = summed(local_bias, "sp")

    partial_x = dot32(grad_query, w_query, ((1,), (1,)))
    partial_x = partial_x + dot32(grad_key, w_key, ((1,), (1,)))
    partial_x = partial_x + dot32(grad_value, w_value, ((1,), (1,)))
    grad_inputs = scattered(partial_x.astype(jnp.bfloat16), "tp")
    return (grad_inputs, grad_w_query, grad_w_key, grad_w_value, grad_bias)


def solution(mesh):
    placed = (
        P("sp", "tp"),
        P(None, "tp"),
        P(None, "tp"),
        P(None, "tp"),
        P(None, "tp"),
        P("sp", "tp"),
    )
    return jax.shard_map(
        local,
        mesh=mesh,
        in_specs=placed,
        out_specs=(P("sp", "tp"), P("sp", "tp"), P("sp", "tp"), P("sp", "tp"), P(None, "tp")),
        check_vma=False,
    )
```

profile of v0, /device:TPU:0, one launch (start us, length us, event | category | flops | bytes accessed | tf_op | source)
XLA Modules:
  0.0 287.2 jit_solution(16715388423824174866)
XLA Ops:
  8.0 1.9 convolution_bitcast_fusion
  10.5 46.7 %all-gather.2.cloned.1.call-done.x_ref = bf16[512,3072]{1,0:T(8,128)(2,1)} async-done(((bf16[512,1536]{1,0:T(8,128)(2,1)}), bf16[512,3072]{1,0:T(8,128)(2,1)}) %all-gather.2.cloned.1.call-update) | async-done | bytes 3145744 | tf_op jit(solution)/shard_map/all_gather | solution.py:209
  57.2 6.0 %convolution_convert_fusion.1.k_ref = bf16[512,768]{1,0:T(8,128)(2,1)S(1)} fusion(bf16[512,3072]{1,0:T(8,128)(2,1)} %all-gather.2.cloned.1.call-done.x_ref, bf16[3072,768]{1,0:T(8,128)(2,1)} %param.11), kind=kOutput, calls=%fused_computation.3 | convolution fusion | flops 2416312320 | bytes 8650752 | tf_op jit(solution)/shard_map/dot_general | solution.py:30
  63.3 2.0 collective-permute-start
  65.3 4.9 %convolution_convert_fusion.v_ref = bf16[512,768]{1,0:T(8,128)(2,1)S(1)} fusion(bf16[512,3072]{1,0:T(8,128)(2,1)S(1)} %copy-done.7, bf16[3072,768]{1,0:T(8,128)(2,1)} %param.12), kind=kOutput, calls=%fused_computation.2 | convolution fusion | flops 2416312320 | bytes 8650752 | tf_op jit(solution)/shard_map/dot_general | solution.py:30
  70.3 3.7 %collective-permute-start.1 = (bf16[256,768]{1,0:T(8,128)(2,1)S(1)}, bf16[256,768]{1,0:T(8,128)(2,1)S(1)}, u32[]{:S(2)}, u32[]{:S(2)}) collective-permute-start(bf16[256,768]{1,0:T(8,128)(2,1)S(1)} %slice.39), channel_id=1, source_target_pairs={{0,2},{2,4},{4,6},{6,8},{8,10},{10,12},{12,14},{14,16},{16,18},{18... | collective-permute-start | bytes 1179656 | tf_op jit(solution)/shard_map/ppermute | solution.py:26
  74.0 3.5 %convolution_convert_fusion.2.q_ref = bf16[512,768]{1,0:T(8,128)(2,1)} fusion(bf16[512,3072]{1,0:T(8,128)(2,1)S(1)} %copy-done.7, bf16[3072,768]{1,0:T(8,128)(2,1)S(1)} %bitcast.17), kind=kOutput, calls=%fused_computation.4 | convolution fusion | flops 2416312320 | bytes 8650752 | tf_op jit(solution)/shard_map/dot_general | solution.py:30
  78.7 25.0 %attention.1 = (bf16[512,768]{1,0:T(8,128)(2,1)}, bf16[256,768]{1,0:T(8,128)(2,1)}, f32[512,768]{1,0:T(8,128)}, bf16[256,768]{1,0:T(8,128)(2,1)}, f32[512,768]{1,0:T(8,128)}, /*index=5*/f32[6,2,512]{2,1,0:T(2,128)}) custom-call(f32[6,2,512]{2,1,0:T(2,128)} %reshape.22.line_ref, f32[640,256]{1,0:T(8,128)} %broadcast_in_dim.16.keep_ref, ...), custom_call_target="tpu_custom_call" | custom-call | flops 3019898880 | bytes 7864320 | tf_op jit(solution)/shard_map/attention/pallas_call | solution.py:117
  112.4 12.0 %weight_product.1 = bf16[3072,2304]{1,0:T(8,128)(2,1)} custom-call(bf16[512,3072]{1,0:T(8,128)(2,1)} %all-gather.2.cloned.1.call-done.x_ref, bf16[512,768]{1,0:T(8,128)(2,1)} %get-tuple-element.11.refs_0_, bf16[512,768]{1,0:T(8,128)(2,1)} %pad_maximum_fusion.refs_1_, bf16[512,768]{1,0:T(8,128)(2,1)} %pad_maximum_fusion.1.refs_2_), custom_call_target="tpu_custom_call" | custom-call | flops 7247757312 | bytes 19660800 | tf_op jit(solution)/shard_map/weight_product/pallas_call | solution.py:165
  124.4 4.5 %fusion.2 = f32[512,3072]{1,0:T(8,128)S(1)} fusion(bf16[3072,768]{1,0:T(8,128)(2,1)} %param.11, bf16[256,768]{1,0:T(8,128)(2,1)S(1)} %add_convert_fusion.3, bf16[256,768]{1,0:T(8,128)(2,1)S(1)} %slice.50), kind=kOutput, calls=%fused_computation.16 | convolution fusion | flops 2417491968 | bytes 11796480 | tf_op jit(solution)/shard_map/dot_general | solution.py:30
  129.0 4.6 %fusion.1 = f32[512,3072]{1,0:T(8,128)S(1)} fusion(bf16[3072,768]{1,0:T(8,128)(2,1)} %param.12, bf16[256,768]{1,0:T(8,128)(2,1)S(1)} %add_convert_fusion.2, bf16[256,768]{1,0:T(8,128)(2,1)S(1)} %slice.49), kind=kOutput, calls=%fused_computation.15 | convolution fusion | flops 2417491968 | bytes 11796480 | tf_op jit(solution)/shard_map/dot_general | solution.py:30
  133.6 5.2 %add_convert_fusion = bf16[512,3072]{1,0:T(8,128)(2,1)S(1)} fusion(f32[512,3072]{1,0:T(8,128)S(1)} %fusion.1, f32[512,3072]{1,0:T(8,128)S(1)} %fusion.2, bf16[512,768]{1,0:T(8,128)(2,1)S(1)} %copy-done.3, bf16[3072,768]{1,0:T(8,128)(2,1)} %param.10), kind=kOutput, calls=%fused_computation | convolution fusion | flops 2420637696 | bytes 21233664 | tf_op jit(solution)/shard_map/dot_general | solution.py:30
  140.7 1.8 fusion.4
  142.4 8.6 %collective-permute-start.5 = (f32[320,12]{0,1:T(8,128)S(1)}, f32[320,12]{0,1:T(8,128)S(1)}, u32[]{:S(2)}, u32[]{:S(2)}) collective-permute-start(f32[320,12]{0,1:T(8,128)S(1)} %fusion.4), channel_id=1, source_target_pairs={{0,2},{2,0},{4,6},{6,4},{8,10},{10,8},{12,14},{14,12},{16,18},{18,... | collective-permute-start | bytes 46088 | tf_op jit(solution)/shard_map/ppermute | solution.py:187
  151.9 2.7 collective-permute-start.6
  154.6 1.8 collective-permute-done.6
  156.4 1.5 collective-permute-start.7
  157.9 2.3 collective-permute-done.7
  160.3 2.4 collective-permute-start.8
  162.7 2.3 collective-permute-done.8
  165.6 3.9 %collective-permute-done.4 = bf16[512,1536]{1,0:T(8,128)(2,1)} collective-permute-done((bf16[512,1536]{1,0:T(8,128)(2,1)}, bf16[512,1536]{1,0:T(8,128)(2,1)}, u32[]{:S(2)}, u32[]{:S(2)}) %collective-permute-start.4) | collective-permute-done | bytes 1572896 | tf_op jit(solution)/shard_map/ppermute | solution.py:199
  169.5 3.0 %add_convert_fusion.1 = bf16[512,1536]{1,0:T(8,128)(2,1)} fusion(bf16[512,1536]{1,0:T(8,128)(2,1)} %collective-permute-done.4, bf16[512,3072]{1,0:T(8,128)(2,1)S(1)} %add_convert_fusion, s32[]{:T(128)S(6)} %select_n.22), kind=kLoop, calls=%fused_computation.1 | loop fusion | flops 3145728 | bytes 4718596 | tf_op jit(solution)/shard_map/convert_element_type | solution.py:201
  172.5 105.5 %reduce-scatter.2.cloned.1.call-done = bf16[192,2304]{1,0:T(8,128)(2,1)} async-done(((bf16[3072,2304]{1,0:T(8,128)(2,1)}), bf16[192,2304]{1,0:T(8,128)(2,1)}) %reduce-scatter.2.cloned.1.call-update) | async-done | bytes 884752 | tf_op jit(solution)/shard_map/reduce_scatter | solution.py:244
  278.0 2.4 fusion.3
  (54 shorter events, 14.6 us)
Async XLA Ops:
  7.2 0.8 copy-start
  7.2 50.0 %all-gather.2.cloned.1.call-start = ((), (), s32[]{:S(2)}) async-start(), calls=%async_computation.1 | async-start | bytes 4718592 | tf_op jit(solution)/shard_map/all_gather | solution.py:209
  7.9 270.1 %reduce-scatter.2.cloned.1.call-start = ((), (), s32[]{:S(2)}) async-start(), calls=%async_computation.2 | async-start | bytes 15040512 | tf_op jit(solution)/shard_map/reduce_scatter | solution.py:244
  57.2 8.1 %copy-start.7 = (bf16[512,3072]{1,0:T(8,128)(2,1)S(1)}, bf16[512,3072]{1,0:T(8,128)(2,1)}, u32[]{:S(2)}) copy-start(bf16[512,3072]{1,0:T(8,128)(2,1)} %all-gather.2.cloned.1.call-done.x_ref) | copy-start | bytes 9437188
  63.2 7.0 %copy-start.4 = (bf16[512,768]{1,0:T(8,128)(2,1)}, bf16[512,768]{1,0:T(8,128)(2,1)S(1)}, u32[]{:S(2)}) copy-start(bf16[512,768]{1,0:T(8,128)(2,1)S(1)} %convolution_convert_fusion.1.k_ref) | copy-start | bytes 2359300
  63.2 10.8 %slice-start = ((s8[4718592]{0:T(1024)(128)(4,1)}), s8[4194304]{0:T(1024)(128)(4,1)S(1)}, s32[]{:S(2)}) async-start(s8[4718592]{0:T(1024)(128)(4,1)} %bitcast.16), calls=%async_computation.3 | async-start | bytes 8388608
  63.3 10.7 %slice-start.1 = ((s8[4718592]{0:T(1024)(128)(4,1)}), s8[524288]{0:T(1024)(128)(4,1)S(1)}, s32[]{:S(2)}) async-start(s8[4718592]{0:T(1024)(128)(4,1)} %bitcast.16), calls=%async_computation.4 | async-start | bytes 1048576
  63.3 14.3 %collective-permute-start = (bf16[256,768]{1,0:T(8,128)(2,1)S(1)}, bf16[256,768]{1,0:T(8,128)(2,1)S(1)}, u32[]{:S(2)}, u32[]{:S(2)}) collective-permute-start(bf16[256,768]{1,0:T(8,128)(2,1)S(1)} %slice.38), channel_id=1, source_target_pairs={{0,2},{2,4},{4,6},{6,8},{8,10},{10,12},{12,14},{14,16},{16,18},{18... | collective-permute-start | bytes 1179656 | tf_op jit(solution)/shard_map/ppermute | solution.py:26
  70.3 7.3 %copy-start.5 = (bf16[512,768]{1,0:T(8,128)(2,1)}, bf16[512,768]{1,0:T(8,128)(2,1)S(1)}, u32[]{:S(2)}) copy-start(bf16[512,768]{1,0:T(8,128)(2,1)S(1)} %convolution_convert_fusion.v_ref) | copy-start | bytes 2359300
  70.3 7.3 %collective-permute-start.1 = (bf16[256,768]{1,0:T(8,128)(2,1)S(1)}, bf16[256,768]{1,0:T(8,128)(2,1)S(1)}, u32[]{:S(2)}, u32[]{:S(2)}) collective-permute-start(bf16[256,768]{1,0:T(8,128)(2,1)S(1)} %slice.39), channel_id=1, source_target_pairs={{0,2},{2,4},{4,6},{6,8},{8,10},{10,12},{12,14},{14,16},{16,18},{18... | collective-permute-start | bytes 1179656 | tf_op jit(solution)/shard_map/ppermute | solution.py:26
  77.6 1.1 copy-start.8
  77.6 1.1 copy-start.9
  103.6 7.8 %copy-start.2 = (f32[512,768]{1,0:T(8,128)S(1)}, f32[512,768]{1,0:T(8,128)}, u32[]{:S(2)}) copy-start(f32[512,768]{1,0:T(8,128)} %get-tuple-element.14) | copy-start | bytes 4718596
  103.6 5.3 %collective-permute-start.2 = (bf16[256,768]{1,0:T(8,128)(2,1)}, bf16[256,768]{1,0:T(8,128)(2,1)S(1)}, u32[]{:S(2)}, u32[]{:S(2)}) collective-permute-start(bf16[256,768]{1,0:T(8,128)(2,1)} %get-tuple-element.13), channel_id=1, source_target_pairs={{2,0},{4,2},{6,4},{8,6},{10,8},{12,10},{14,12},{16,14},{18,16},{20... | collective-permute-start | bytes 1179656 | tf_op jit(solution)/shard_map/ppermute | solution.py:26
  106.2 5.1 %collective-permute-start.3 = (bf16[256,768]{1,0:T(8,128)(2,1)}, bf16[256,768]{1,0:T(8,128)(2,1)S(1)}, u32[]{:S(2)}, u32[]{:S(2)}) collective-permute-start(bf16[256,768]{1,0:T(8,128)(2,1)} %get-tuple-element.15), channel_id=1, source_target_pairs={{2,0},{4,2},{6,4},{8,6},{10,8},{12,10},{14,12},{16,14},{18,16},{20... | collective-permute-start | bytes 1179656 | tf_op jit(solution)/shard_map/ppermute | solution.py:26
  129.0 4.6 %copy-start.3 = (bf16[512,768]{1,0:T(8,128)(2,1)S(1)}, bf16[512,768]{1,0:T(8,128)(2,1)}, u32[]{:S(2)}) copy-start(bf16[512,768]{1,0:T(8,128)(2,1)} %get-tuple-element.11.refs_0_) | copy-start | bytes 2359300
  138.8 1.8 copy-start.6
  140.1 29.4 %collective-permute-start.4 = (bf16[512,1536]{1,0:T(8,128)(2,1)}, bf16[512,1536]{1,0:T(8,128)(2,1)}, u32[]{:S(2)}, u32[]{:S(2)}) collective-permute-start(bf16[512,1536]{1,0:T(8,128)(2,1)} %constant_dynamic-slice_fusion), channel_id=1, source_target_pairs={{0,1},{1,0},{2,3},{3,2},{4,5},{5,4},{6,7},{7,6},{8,9},{9,8},{10,11... | collective-permute-start | bytes 4718600 | tf_op jit(solution)/shard_map/ppermute | solution.py:199
  142.4 9.5 %collective-permute-start.5 = (f32[320,12]{0,1:T(8,128)S(1)}, f32[320,12]{0,1:T(8,128)S(1)}, u32[]{:S(2)}, u32[]{:S(2)}) collective-permute-start(f32[320,12]{0,1:T(8,128)S(1)} %fusion.4), channel_id=1, source_target_pairs={{0,2},{2,0},{4,6},{6,4},{8,10},{10,8},{12,14},{14,12},{16,18},{18,... | collective-permute-start | bytes 46088 | tf_op jit(solution)/shard_map/ppermute | solution.py:187
  151.9 4.5 %collective-permute-start.6 = (f32[320,12]{0,1:T(8,128)S(1)}, f32[320,12]{0,1:T(8,128)S(1)}, u32[]{:S(2)}, u32[]{:S(2)}) collective-permute-start(f32[320,12]{0,1:T(8,128)S(1)} %add.64), channel_id=1, source_target_pairs={{0,4},{2,6},{4,0},{6,2},{8,12},{10,14},{12,8},{14,10},{16,20},{18,... | collective-permute-start | bytes 46088 | tf_op jit(solution)/shard_map/ppermute | solution.py:187
  156.4 3.8 %collective-permute-start.7 = (f32[320,12]{0,1:T(8,128)S(1)}, f32[320,12]{0,1:T(8,128)S(1)}, u32[]{:S(2)}, u32[]{:S(2)}) collective-permute-start(f32[320,12]{0,1:T(8,128)S(1)} %add.65), channel_id=1, source_target_pairs={{0,8},{2,10},{4,12},{6,14},{8,0},{10,2},{12,4},{14,6},{16,24},{18,... | collective-permute-start | bytes 46088 | tf_op jit(solution)/shard_map/ppermute | solution.py:187
  160.3 4.7 %collective-permute-start.8 = (f32[320,12]{0,1:T(8,128)S(1)}, f32[320,12]{0,1:T(8,128)S(1)}, u32[]{:S(2)}, u32[]{:S(2)}) collective-permute-start(f32[320,12]{0,1:T(8,128)S(1)} %add.66), channel_id=1, source_target_pairs={{0,16},{2,18},{4,20},{6,22},{8,24},{10,26},{12,28},{14,30},{16,0},... | collective-permute-start | bytes 46088 | tf_op jit(solution)/shard_map/ppermute | solution.py:187
  165.0 115.4 %copy-start.1 = (f32[320,12]{0,1:T(8,128)S(1)}, f32[320,12]{0,1:T(8,128)}, u32[]{:S(2)}) copy-start(f32[320,12]{0,1:T(8,128)} %param.13) | copy-start | bytes 46084
Sparse Core Ops, SparseCore 0:
  9.5 47.6 all-gather.1
  124.5 153.4 reduce-scatter.1
where the time goes:
time: 288 us; the launch traced here: 287 us
  waiting for transfers between devices  164 us (57%)
  Pallas kernels  36.9 us (13%)
  matrix products  32.5 us (11%)
  starting transfers between devices  24.5 us (9%)
  between operations  14.3 us (5%)
  local copies, waits for them, and re-layouts  7.85 us (3%)
  other arithmetic  6.82 us (2%)
    reduce_scatter x1, waiting for transfers between devices, local(): lax.psum_scatter(weight_product(whole, (grad_query, grad_key, grad_value)...  105 us
    all_gather x1, waiting for transfers between devices, local(): whole = lax.all_gather(inputs, 'tp', axis=1, tiled=True)  46.7 us
    dot_general x6, matrix products, dot32(): lax.dot_general(a, b, (dims, ((), ())), preferred_element_type=jnp.float32)  28.8 us
    pallas_call x1, Pallas kernels, attention(): pl.pallas_call(attention_body, grid=(pairs,), in_specs=[line_spec, fixed(...  25 us
    ppermute x4, starting transfers between devices, summed(): lax.ppermute(block, axis, [(i, i ^ step) for i in range(size)])  15.2 us
    pallas_call x1, Pallas kernels, weight_product(): pl.pallas_call(weight_body, grid=(features // tile,), in_specs=[pl.BlockS...  12 us
    ppermute x4, starting transfers between devices, passed_along(): return lax.ppermute(block, axis, route)  8.59 us
    ppermute x4, waiting for transfers between devices, summed(): lax.ppermute(block, axis, [(i, i ^ step) for i in range(size)])  7.3 us
  transfers between devices with their start and end apart: 11, of which 8 were waited for; matrix products, arithmetic and copies ran while one was open for 13% of the time, Pallas kernels for 0%

commit v1 on v0

v1 whole, which is shorter than its diff:
```python
import functools

import jax
import jax.numpy as jnp
from jax import lax
from jax.experimental import pallas as pl
from jax.experimental.pallas import tpu as pltpu
from jax.sharding import PartitionSpec as P

HEAD = 64
SEG = 64
LEFT = 4
REL_MAX = 256
LANES = 128
QB = 2 * SEG
HALO = LEFT * SEG
KB = HALO + QB
LINE = 512
UNSEEN = -1e30
CHUNK = 128
TILE = 256
TRIO = 3 * LANES
MESH = pl.DeviceIdType.MESH
BF = jnp.bfloat16
F32 = jnp.float32


def dot32(a, b, dims):
    return lax.dot_general(a, b, (dims, ((), ())), preferred_element_type=F32)


def exact(a, b, dims):
    return lax.dot_general(
        a, b, (dims, ((), ())), precision=lax.Precision.HIGHEST, preferred_element_type=F32
    )


def grid_of(chips):
    depth = 1
    while depth * depth < chips:
        depth *= 2
    return depth, chips // depth


def aligned(index, size):
    return pl.ds(pl.multiple_of(index * size, size), size)


def bias_index(apart):
    return jnp.clip(HALO + apart, 1 - SEG, REL_MAX) + SEG - 1


def step_body(
    sizes,
    x_ref, wq_ref, wk_ref, wv_ref, rel_ref, d_ref,
    gi_ref, dwq_ref, dwk_ref, dwv_ref, gb_ref,
    xw, wcat, xt, xg, zacc, q_s, k_ext, v_ext, d_s, lines, dline, bias, bias_sum, kacc, vacc,
    halo_s, halo_r, dall, rr, rl, pxs, pxr, bslot, brecv,
    w_sem, d_sem, x_sem, xs_sem, xr_sem, gs_sem, gr_sem, gl_sem, ks_sem, kr_sem, hs_sem, hr_sem,
    ys_sem, yr_sem, cs_sem, cr_sem, rs_sem, rv_sem, ls_sem, lv_sem, bs_sem, br_sem, ps_sem, pr_sem,
):
    seq, tps = sizes
    deep, wide = grid_of(seq // 2)
    rows, dloc = x_ref.shape
    pairs = wq_ref.shape[1] // LANES
    ext = HALO + rows
    blocks = rows // QB
    feat = dloc * tps // seq
    group = 2 * wide
    sp = lax.axis_index("sp")
    tp = lax.axis_index("tp")
    core = lax.rem(sp, 2)
    chip = lax.div(sp, 2)
    y = lax.rem(chip, wide)
    z = lax.div(chip, wide)
    mine = y * 2 + core

    def at(zi, yi, ci):
        return ((zi * wide + yi) * 2 + ci, tp)

    def mod(a, n):
        return lax.rem(a + n, n)

    mate = at(z, y, 1 - core)
    ahead, behind = (sp + 1, tp), (sp - 1, tp)
    has_ahead, has_behind = sp + 1 < seq, sp > 0

    greeted = [(sp, mod(tp + k, tps)) for k in range(1, tps)]
    greeted += [(mod(sp + 1, seq), tp), (mod(sp - 1, seq), tp)]
    greeted += [at(z, mod(y + j, wide), mod(core + i, 2)) for j in range(wide) for i in range(2) if i + j]
    greeted += [at(mod(z + 1, deep), y, core), at(mod(z - 1, deep), y, core)]
    steps = seq.bit_length() - 1
    greeted += [(jnp.bitwise_xor(sp, 1 << k), tp) for k in range(steps)]
    barrier = pltpu.get_barrier_semaphore()
    for other in greeted:
        pl.semaphore_signal(barrier, inc=1, device_id=other, device_id_type=MESH)
    pl.semaphore_wait(barrier, len(greeted))

    def remote(src, dst, send, recv, device):
        return pltpu.make_async_remote_copy(
            src_ref=src, dst_ref=dst, send_sem=send, recv_sem=recv,
            device_id=device, device_id_type=MESH,
        )

    chunks = rows // CHUNK
    first = (rows - HALO) // CHUNK
    order = list(range(first, chunks)) + list(range(first))

    def x_copy(k, r):
        part = slice(r * CHUNK, (r + 1) * CHUNK)
        return remote(
            x_ref.at[part, :], xw.at[part, aligned(tp, dloc)],
            xs_sem.at[k - 1, r], xr_sem.at[k - 1, r], (sp, mod(tp + k, tps)),
        )

    for r in order:
        for k in range(1, tps):
            x_copy(k, r).start()
    own_x = pltpu.make_async_copy(x_ref, xw.at[:, aligned(tp, dloc)], x_sem)
    own_x.start()
    for p in range(pairs):
        for j, w_ref in enumerate((wq_ref, wk_ref, wv_ref)):
            pltpu.make_async_copy(
                w_ref.at[:, p * LANES : (p + 1) * LANES],
                wcat.at[:, p * TRIO + j * LANES : p * TRIO + (j + 1) * LANES], w_sem,
            ).start()
    for p in range(pairs):
        pltpu.make_async_copy(
            d_ref.at[:, p * LANES : (p + 1) * LANES], d_s.at[p], d_sem
        ).start()
    own_x.wait()

    def turn(t, r):
        part = slice(r * CHUNK, (r + 1) * CHUNK)

        @pl.loop(0, dloc // TILE)
        def _(f):
            cols = aligned(t * (dloc // TILE) + f, TILE)
            xt[cols, part] = xw[part, cols].T

    zparts = deep // tps

    def share(t, low, high):
        for j in range(wide):
            for i in range(2):
                for q in range(zparts):
                    zb = t * zparts + q
                    y2, c2 = mod(y + j, wide), mod(core + i, 2)
                    src = xt.at[aligned((zb * wide + y2) * 2 + c2, feat), low:high]
                    cols = pl.ds(pl.multiple_of(mine * rows + low, CHUNK), high - low)
                    dst = xg.at[aligned(zb, feat), cols]
                    if i + j:
                        remote(src, dst, gs_sem, gr_sem, at(z, y2, c2)).start()
                    else:
                        pltpu.make_async_copy(src, dst, gl_sem).start()

    for r in range(chunks):
        turn(tp, r)
    share(tp, 0, rows)

    pltpu.make_async_copy(wcat, wcat, w_sem).wait()

    @pl.loop(0, pairs)
    def _(p):
        zacc[p, :rows, :] = dot32(
            xw[:, aligned(tp, dloc)], wcat[aligned(tp, dloc), aligned(p, TRIO)], ((1,), (0,))
        )

    @pl.when(sp == 0)
    def _():
        k_ext[:, :HALO, :] = jnp.zeros((pairs, HALO, LANES), BF)
        v_ext[:, :HALO, :] = jnp.zeros((pairs, HALO, LANES), BF)

    spot = lax.broadcasted_iota(jnp.int32, (rel_ref.shape[1], LINE), 1)
    entry = lax.broadcasted_iota(jnp.int32, (rel_ref.shape[1], LINE), 0)
    apart = jnp.where(spot < QB, spot, spot - LINE)
    picked = exact(rel_ref[...], jnp.where(bias_index(apart) == entry, 1.0, 0.0), ((1,), (0,)))
    for n in range(2 * pairs):
        lines[n] = picked[n : n + 1, :]

    def halo_copy(ref, n):
        return remote(
            ref.at[:, rows : rows + HALO, :], ref.at[:, :HALO, :],
            ks_sem.at[n], kr_sem.at[n], ahead,
        )

    for n, r in enumerate(order):
        part = slice(r * CHUNK, (r + 1) * CHUNK)
        for k in range(1, tps):
            x_copy(k, r).wait_recv()

        @pl.loop(0, pairs)
        def _(p):
            total = zacc[p, part, :]
            for k in range(1, tps):
                t = mod(tp - k, tps)
                total = total + dot32(
                    xw[part, aligned(t, dloc)], wcat[aligned(t, dloc), aligned(p, TRIO)],
                    ((1,), (0,)),
                )
            low = total.astype(BF)
            q_s[p, part, :] = low[:, :LANES]
            k_ext[p, HALO + r * CHUNK : HALO + (r + 1) * CHUNK, :] = low[:, LANES : 2 * LANES]
            v_ext[p, HALO + r * CHUNK : HALO + (r + 1) * CHUNK, :] = low[:, 2 * LANES :]

        if n == chunks - first - 1:
            @pl.when(has_ahead)
            def _():
                halo_copy(k_ext, 0).start()
                halo_copy(v_ext, 1).start()

        for k in range(1, tps):
            t = mod(tp - k, tps)
            turn(t, r)
            share(t, r * CHUNK, (r + 1) * CHUNK)

    pltpu.make_async_copy(d_s, d_s, d_sem).wait()

    @pl.when(has_behind)
    def _():
        halo_copy(k_ext, 0).wait_recv()
        halo_copy(v_ext, 1).wait_recv()

    key_row = lax.broadcasted_iota(jnp.int32, (KB, QB), 0)
    query_row = lax.broadcasted_iota(jnp.int32, (KB, QB), 1)
    lane = lax.broadcasted_iota(jnp.int32, (QB, LANES), 1)
    scale = HEAD ** (-0.5)
    zero = jnp.zeros((QB, LANES), BF)
    own_rows = aligned(mine, rows)

    def stacked(part):
        return jnp.concatenate(
            [jnp.where(lane < HEAD, part, zero), jnp.where(lane < HEAD, zero, part)], axis=0
        )

    def grad_halo(p):
        return remote(halo_s.at[p], halo_r.at[p], hs_sem.at[p], hr_sem.at[p], behind)

    def attend(p):
        slot = lax.rem(p, 2)
        offset = key_row - jnp.where(query_row < SEG, 0, SEG)
        seen = (offset >= 0) & (offset < HALO + SEG)
        for half in range(2):
            line = jnp.broadcast_to(lines[2 * p + half], (KB, LINE))
            skewed = pltpu.roll(line, 0, 1, stride=1, stride_axis=0)[:, :QB]
            bias[:, half * QB : (half + 1) * QB] = jnp.where(seen, skewed, UNSEEN)
        kacc[slot] = jnp.zeros((ext, LANES), F32)
        vacc[slot] = jnp.zeros((ext, LANES), F32)
        bias_sum[...] = jnp.zeros_like(bias_sum)
        for block in range(blocks):
            keys = slice(block * QB, block * QB + KB)
            part = slice(block * QB, (block + 1) * QB)
            q2 = stacked(q_s[p, part, :] * BF(scale))
            d2 = stacked(d_s[p, part, :])
            k = k_ext[p, keys, :]
            v = v_ext[p, keys, :]
            score = dot32(k, q2, ((1,), (1,))) + bias[...]
            if block * QB < HALO:
                row = lax.broadcasted_iota(jnp.int32, (KB, 1), 0) + block * QB
                score = score + jnp.where((row < HALO) & (sp == 0), UNSEEN, 0.0)
            top = jnp.max(score, axis=0, keepdims=True)
            power = jnp.exp(score - top)
            prob = power * (1.0 / jnp.sum(power, axis=0, keepdims=True))
            prob_low = prob.astype(BF)
            grad_prob = dot32(v, d2, ((1,), (1,)))
            delta = jnp.sum(prob_low.astype(F32) * grad_prob, axis=0, keepdims=True)
            dscore = prob * (grad_prob - delta)
            bias_sum[...] += dscore
            dscore_low = dscore.astype(BF)
            vacc[slot, keys, :] += dot32(prob_low, d2, ((1,), (0,)))
            kacc[slot, keys, :] += dot32(dscore_low, q2, ((1,), (0,)))
            dq_t = dot32(k, dscore_low, ((0,), (0,)))
            dq_t = jnp.concatenate([dq_t[:HEAD, :QB], dq_t[HEAD:, QB:]], axis=0)
            dq = (dq_t.T * scale).astype(BF)
            xw[part, aligned(p * 3, LANES)] = dq
            dall[p, pl.ds(pl.multiple_of(mine * rows + block * QB, QB), QB), :LANES] = dq
        halo_s[p, 0] = kacc[slot, :HALO, :].astype(BF)
        halo_s[p, 1] = vacc[slot, :HALO, :].astype(BF)

        @pl.when(has_behind)
        def _():
            grad_halo(p).start()

        flip_row = lax.broadcasted_iota(jnp.int32, (KB, KB), 0)
        flip_col = lax.broadcasted_iota(jnp.int32, (KB, KB), 1)
        flip = jnp.where(flip_row + flip_col == KB - 1, 1.0, 0.0)
        flipped = exact(flip, bias_sum[...], ((1,), (0,)))
        for half in range(2):
            part = flipped[:, half * QB : (half + 1) * QB]
            spread = jnp.concatenate([part, jnp.zeros((KB, LINE - QB), F32)], axis=1)
            skewed = pltpu.roll(spread, 0, 1, stride=1, stride_axis=0)
            dline[2 * p + half] = jnp.sum(skewed, axis=0, keepdims=True)

    def to_wide(p, k):
        view = dall.at[p, own_rows, :]
        return remote(
            view, view, ys_sem.at[p, k - 1], yr_sem.at[p, k - 1], at(z, mod(y + k, wide), core)
        )

    def to_mate(p, k):
        owner = aligned(mod(y - k, wide) * 2 + core, rows)
        view = dall.at[p, owner, :]
        return remote(view, view, cs_sem.at[p, k], cr_sem.at[p, k], mate)

    def settle(p):
        slot = lax.rem(p, 2)

        @pl.when(has_ahead)
        def _():
            grad_halo(p).wait_recv()
            kacc[slot, rows:, :] += halo_r[p, 0].astype(F32)
            vacc[slot, rows:, :] += halo_r[p, 1].astype(F32)

        for j, total in ((1, kacc), (2, vacc)):
            low = total[slot, HALO:, :].astype(BF)
            xw[:, aligned(p * 3 + j, LANES)] = low
            dall[p, own_rows, j * LANES : (j + 1) * LANES] = low
        for k in range(1, wide):
            to_wide(p, k).start()
        to_mate(p, 0).start()

    def forward(p):
        for k in range(1, wide):
            to_wide(p, k).wait_recv()
            to_mate(p, k).start()

    def block_of(b):
        return slice(b * feat, (b + 1) * feat)

    def to_right(p, b):
        return remote(
            rr.at[p, b], rr.at[p, b], rs_sem.at[p, b], rv_sem.at[p, b], at(z + 1, y, core)
        )

    def to_left(p, b):
        return remote(
            rl.at[p, b], rl.at[p, b], ls_sem.at[p, b], lv_sem.at[p, b], at(z - 1, y, core)
        )

    def hop(p, h):
        @pl.when(z == h)
        def _():
            for b in range(deep - 1, h, -1):
                total = zacc[p, block_of(b), :]
                if h:
                    to_right(p, b).wait_recv()
                    total = total + rr[p, b].astype(F32)
                rr[p, b] = total.astype(BF)
                to_right(p, b).start()

        @pl.when(z == deep - 1 - h)
        def _():
            for b in range(0, deep - 1 - h):
                total = zacc[p, block_of(b), :]
                if h:
                    to_left(p, b).wait_recv()
                    total = total + rl[p, b].astype(F32)
                rl[p, b] = total.astype(BF)
                to_left(p, b).start()

    def product(p):
        for k in range(wide):
            to_mate(p, k).wait_recv()

        @pl.when(p == 0)
        def _():
            some = xg.at[:, : (group - 1) * rows]
            pltpu.make_async_copy(some, some, gr_sem).wait()
            some = xg.at[:, :rows]
            pltpu.make_async_copy(some, some, gl_sem).wait()

        zacc[p, : deep * feat, :] = dot32(xg[...], dall[p], ((1,), (0,)))
        hop(p, 0)

    def finish(p):
        me = aligned(z, feat)

        @pl.when(z > 0)
        def _():
            to_right(p, z).wait_recv()
            zacc[p, me, :] += rr[p, z].astype(F32)

        @pl.when(z < deep - 1)
        def _():
            to_left(p, z).wait_recv()
            zacc[p, me, :] += rl[p, z].astype(F32)

        total = zacc[p, me, :]
        for j, ref in enumerate((dwq_ref, dwk_ref, dwv_ref)):
            ref[:, aligned(p, LANES)] = total[:, j * LANES : (j + 1) * LANES]

    def bias_copy(k):
        return remote(
            bslot.at[k], brecv.at[k], bs_sem.at[k], br_sem.at[k],
            (jnp.bitwise_xor(sp, 1 << k), tp),
        )

    def bias_step(k):
        if k:
            bias_copy(k - 1).wait_recv()
            bslot[k] = bslot[k - 1] + brecv[k - 1]
        else:
            bslot[0] = jnp.concatenate([dline[n] for n in range(2 * pairs)], axis=0)
        if k < steps:
            bias_copy(k).start()

    tiles = dloc // TILE
    away = (tps - 1) * tiles

    def px_copy(j):
        return remote(
            pxs.at[j], pxr.at[j], ps_sem, pr_sem, (sp, mod(tp + 1 + lax.div(j, tiles), tps))
        )

    def input_tile(j):
        place = mod(tp + 1 + lax.div(j, tiles), tps) * tiles + lax.rem(j, tiles)
        low = dot32(
            xw[:, : pairs * TRIO], wcat[aligned(place, TILE), :], ((1,), (1,))
        ).astype(BF)

        @pl.when(j < away)
        def _():
            pxs[j] = low
            px_copy(j).start()

        @pl.when(j >= away)
        def _():
            gi_ref[:, aligned(j - away, TILE)] = low

    hops = deep - 2
    lag_end = 5 + hops
    rounds = pairs + lag_end + 1
    late = rounds - (pairs + 1)
    per = -(-tps * tiles // late)

    def staged(i, lag, stage):
        p = i - lag

        @pl.when((p >= 0) & (p < pairs))
        def _():
            stage(p)

    @pl.loop(0, rounds)
    def _(i):
        staged(i, 0, attend)
        staged(i, 1, settle)
        staged(i, 3, forward)
        staged(i, 4, product)
        for h in range(1, hops + 1):
            staged(i, 4 + h, functools.partial(hop, h=h))
        staged(i, lag_end, finish)
        for k in range(steps + 1):
            @pl.when(i == pairs + k)
            def _():
                bias_step(k)

        @pl.when(i > pairs)
        def _():
            @pl.loop(0, per)
            def _(n):
                j = (i - pairs - 1) * per + n

                @pl.when(j < tps * tiles)
                def _():
                    input_tile(j)

    spot = lax.broadcasted_iota(jnp.int32, (rel_ref.shape[1], LINE), 1)
    back = bias_index(spot - (KB - 1))
    entry = lax.broadcasted_iota(jnp.int32, (rel_ref.shape[1], LINE), 0)
    gb_ref[...] = exact(bslot[steps], jnp.where(back == entry, 1.0, 0.0), ((1,), (1,)))

    pltpu.make_async_copy(pxr, pxr, pr_sem).wait()
    for n in range(tiles):
        cols = slice(n * TILE, (n + 1) * TILE)
        total = gi_ref[:, cols].astype(F32)
        for k in range(1, tps):
            total = total + pxr[(k - 1) * tiles + n].astype(F32)
        gi_ref[:, cols] = total.astype(BF)

    pltpu.make_async_copy(pxs, pxs, ps_sem).wait()
    for r in order:
        for k in range(1, tps):
            x_copy(k, r).wait_send()
    some = xg.at[:, : (group - 1) * rows]
    pltpu.make_async_copy(some, some, gs_sem).wait()

    @pl.when(has_ahead)
    def _():
        halo_copy(k_ext, 0).wait_send()
        halo_copy(v_ext, 1).wait_send()

    for k in range(steps):
        bias_copy(k).wait_send()

    @pl.loop(0, pairs)
    def _(p):
        @pl.when(has_behind)
        def _():
            grad_halo(p).wait_send()

        for k in range(1, wide):
            to_wide(p, k).wait_send()
        for k in range(wide):
            to_mate(p, k).wait_send()
        for b in range(deep):
            @pl.when(z < b)
            def _():
                to_right(p, b).wait_send()

            @pl.when(z > b)
            def _():
                to_left(p, b).wait_send()


def local(sizes, inputs, w_query, w_key, w_value, rel_bias, d_out):
    seq, tps = sizes
    deep, wide = grid_of(seq // 2)
    rows, dloc = inputs.shape
    full, width = w_query.shape
    pairs = width // LANES
    ext = HALO + rows
    feat = full // seq
    group = 2 * wide
    tiles = dloc // TILE
    steps = seq.bit_length() - 1
    chunks = rows // CHUNK
    heads = rel_bias.shape[1]
    sds = jax.ShapeDtypeStruct
    vm = pltpu.VMEM
    dma = pltpu.SemaphoreType.DMA
    hbm = pl.BlockSpec(memory_space=pl.ANY)
    on_chip = pl.BlockSpec(memory_space=pltpu.VMEM)
    out = pl.pallas_call(
        functools.partial(step_body, sizes),
        in_specs=[hbm, hbm, hbm, hbm, on_chip, hbm],
        out_specs=[on_chip] * 5,
        out_shape=[
            sds((rows, dloc), BF),
            sds((feat, width), F32), sds((feat, width), F32), sds((feat, width), F32),
            sds((heads, rel_bias.shape[0]), F32),
        ],
        scratch_shapes=[
            vm((rows, full), BF),
            vm((full, pairs * TRIO), BF),
            vm((full, rows), BF),
            vm((deep * feat, group * rows), BF),
            vm((pairs, max(deep * feat, rows), TRIO), F32),
            vm((pairs, rows, LANES), BF),
            vm((pairs, ext, LANES), BF),
            vm((pairs, ext, LANES), BF),
            vm((pairs, rows, LANES), BF),
            vm((2 * pairs, 1, LINE), F32),
            vm((2 * pairs, 1, LINE), F32),
            vm((KB, 2 * QB), F32),
            vm((KB, 2 * QB), F32),
            vm((2, ext, LANES), F32),
            vm((2, ext, LANES), F32),
            vm((pairs, 2, HALO, LANES), BF),
            vm((pairs, 2, HALO, LANES), BF),
            vm((pairs, group * rows, TRIO), BF),
            vm((pairs, deep, feat, TRIO), BF),
            vm((pairs, deep, feat, TRIO), BF),
            vm(((tps - 1) * tiles, rows, TILE), BF),
            vm(((tps - 1) * tiles, rows, TILE), BF),
            vm((steps + 1, 2 * pairs, LINE), F32),
            vm((steps, 2 * pairs, LINE), F32),
            dma(()), dma(()), dma(()),
            dma((tps - 1, chunks)), dma((tps - 1, chunks)),
            dma(()), dma(()), dma(()),
            dma((2,)), dma((2,)),
            dma((pairs,)), dma((pairs,)),
            dma((pairs, wide - 1)), dma((pairs, wide - 1)),
            dma((pairs, wide)), dma((pairs, wide)),
            dma((pairs, deep)), dma((pairs, deep)),
            dma((pairs, deep)), dma((pairs, deep)),
            dma((steps,)), dma((steps,)),
            dma(()), dma(()),
        ],
        compiler_params=pltpu.CompilerParams(
            collective_id=0, has_side_effects=True, vmem_limit_bytes=67043328
        ),
        name="whole_step",
    )(inputs, w_query, w_key, w_value, rel_bias.T, d_out)
    return out[0], out[1], out[2], out[3], out[4].T


def solution(mesh):
    placed = (
        P("sp", "tp"),
        P(None, "tp"),
        P(None, "tp"),
        P(None, "tp"),
        P(None, "tp"),
        P("sp", "tp"),
    )
    sizes = (mesh.shape["sp"], mesh.shape["tp"])
    return jax.shard_map(
        functools.partial(local, sizes),
        mesh=mesh,
        in_specs=placed,
        out_specs=(P("sp", "tp"), P("sp", "tp"), P("sp", "tp"), P("sp", "tp"), P(None, "tp")),
        check_vma=False,
    )
```

time: 288 us -> 171 us (0.59)
  waiting for transfers between devices: 164 us -> 0 us
  Pallas kernels: 36.9 us -> 163 us
  matrix products: 32.5 us -> 0 us
  starting transfers between devices: 24.5 us -> 0 us
  between operations: 14.3 us -> 0.67 us
  other arithmetic: 6.82 us -> 0 us
    pallas_call x2 -> x1, Pallas kernels: 36.9 us -> 163 us  [local(): pl.pallas_call(functools.partial(step_body, sizes), in_specs=[hbm, hbm, h...]
    reduce_scatter x1 -> x0, waiting for transfers between devices: 105 us -> none  [local(): lax.psum_scatter(weight_product(whole, (grad_query, grad_key, grad_value)...]
    all_gather x1 -> x0, waiting for transfers between devices: 46.7 us -> none  [local(): whole = lax.all_gather(inputs, 'tp', axis=1, tiled=True)]
    dot_general x8 -> x0, matrix products: 32.5 us -> none  [the longest x6 28.8 us: dot32(): lax.dot_general(a, b, (dims, ((), ())), preferred_element_type=jnp.float32)]
    ppermute x9 -> x0, starting transfers between devices: 24.4 us -> none  [the longest x4 15.2 us: summed(): lax.ppermute(block, axis, [(i, i ^ step) for i in range(size)])]
    ppermute x9 -> x0, waiting for transfers between devices: 11.5 us -> none  [the longest x4 7.3 us: summed(): lax.ppermute(block, axis, [(i, i ^ step) for i in range(size)])]
    unnamed x24 -> x11, local copies, waits for them, and re-layouts: 0.07 us -> 6.91 us
    slice x5 -> x0, local copies, waits for them, and re-layouts: 4.79 us -> none  [the longest x1 2.38 us: local(): grad_w_value = weight_grads[:, 2 * width:]]
  transfers between devices with their start and end apart: 11 -> 0, of which waited for: 8 -> 0; matrix products, arithmetic and copies ran while one was open for 13% -> 0% of each run, Pallas kernels for 0% -> 0%
where the time goes in v1:
time: 171 us; the launch traced here: 170 us
  Pallas kernels  163 us (95%)
  local copies, waits for them, and re-layouts  6.91 us (4%)
    pallas_call x1, Pallas kernels, local(): pl.pallas_call(functools.partial(step_body, sizes), in_specs=[hbm, hbm, h...  163 us
    unnamed x11, local copies, waits for them, and re-layouts  6.91 us

profile of v1, /device:TPU:0, one launch (start us, length us, event | category | flops | bytes accessed | tf_op | source)
XLA Modules:
  0.0 170.4 jit_solution(5687231800246601135)
XLA Ops:
  0.6 162.8 %whole_step.1 = (bf16[512,1536]{1,0:T(8,128)(2,1)}, f32[192,768]{1,0:T(8,128)}, f32[192,768]{1,0:T(8,128)}, f32[192,768]{1,0:T(8,128)}, f32[12,320]{1,0:T(8,128)}) custom-call(bf16[512,1536]{1,0:T(8,128)(2,1)} %x_ref.1, bf16[3072,768]{1,0:T(8,128)(2,1)} %wq_ref.1, bf16[3072,768]{1,0:T(8,128)(2,1)} %wk_ref.1, bf16[3072,768]{1,0:T(8,128)(2,1)} %wv_ref.1, ...), custom_call_target="tpu_custom_call" | custom-call | tf_op jit(solution)/shard_map/whole_step/pallas_call | solution.py:533
  163.5 0.0 copy-start.1
  163.5 0.0 copy-start
  163.5 0.0 copy-start.2
  163.5 2.7 %copy.16 = bf16[512,1536]{1,0:T(8,128)(2,1)} copy(bf16[512,1536]{1,0:T(8,128)(2,1)} %get-tuple-element.20) | data formatting | bytes 3145728
  166.2 1.9 %copy.17 = f32[192,768]{1,0:T(8,128)} copy(f32[192,768]{1,0:T(8,128)} %get-tuple-element.21) | data formatting | bytes 1179648
  168.2 0.0 copy-done.1
  168.2 0.8 copy.18
  169.0 0.0 copy-done
  169.0 0.8 copy.19
  169.8 0.0 copy-done.2
  169.8 0.6 copy.20
Async XLA Ops:
  163.5 4.7 %copy-start.1 = (f32[192,768]{1,0:T(8,128)S(1)}, f32[192,768]{1,0:T(8,128)}, u32[]{:S(2)}) copy-start(f32[192,768]{1,0:T(8,128)} %get-tuple-element.22) | copy-start | bytes 1769476
  163.5 5.5 %copy-start = (f32[192,768]{1,0:T(8,128)S(1)}, f32[192,768]{1,0:T(8,128)}, u32[]{:S(2)}) copy-start(f32[192,768]{1,0:T(8,128)} %get-tuple-element.23) | copy-start | bytes 1769476
  163.5 6.3 %copy-start.2 = (f32[12,320]{1,0:T(8,128)S(1)}, f32[12,320]{1,0:T(8,128)}, u32[]{:S(2)}) copy-start(f32[12,320]{1,0:T(8,128)} %get-tuple-element.14) | copy-start | bytes 46084

commit v2 on v1

--- a/solution.py
+++ b/solution.py
@@ -55,10 +55,12 @@
     x_ref, wq_ref, wk_ref, wv_ref, rel_ref, d_ref,
     gi_ref, dwq_ref, dwk_ref, dwv_ref, gb_ref,
     xw, wcat, xt, xg, zacc, q_s, k_ext, v_ext, d_s, lines, dline, bias, bias_sum, kacc, vacc,
-    halo_s, halo_r, dall, rr, rl, pxs, pxr, bslot, brecv,
+    halo_s, halo_r, all_q, all_kv, right_q, right_kv, left_q, left_kv, pxs, pxr, near, far,
     w_sem, d_sem, x_sem, xs_sem, xr_sem, gs_sem, gr_sem, gl_sem, ks_sem, kr_sem, hs_sem, hr_sem,
     ys_sem, yr_sem, cs_sem, cr_sem, rs_sem, rv_sem, ls_sem, lv_sem, bs_sem, br_sem, ps_sem, pr_sem,
 ):
+    alls, rights, lefts = (all_q, all_kv), (right_q, right_kv), (left_q, left_kv)
+    lanes = (slice(0, LANES), slice(LANES, TRIO))
     seq, tps = sizes
     deep, wide = grid_of(seq // 2)
     rows, dloc = x_ref.shape
@@ -88,34 +90,11 @@
     greeted = [(sp, mod(tp + k, tps)) for k in range(1, tps)]
     greeted += [(mod(sp + 1, seq), tp), (mod(sp - 1, seq), tp)]
     greeted += [at(z, mod(y + j, wide), mod(core + i, 2)) for j in range(wide) for i in range(2) if i + j]
-    greeted += [at(mod(z + 1, deep), y, core), at(mod(z - 1, deep), y, core)]
-    steps = seq.bit_length() - 1
-    greeted += [(jnp.bitwise_xor(sp, 1 << k), tp) for k in range(steps)]
+    greeted += [at(mod(z + k, deep), y, core) for k in range(1, deep)]
     barrier = pltpu.get_barrier_semaphore()
     for other in greeted:
         pl.semaphore_signal(barrier, inc=1, device_id=other, device_id_type=MESH)
-    pl.semaphore_wait(barrier, len(greeted))
-
-    def remote(src, dst, send, recv, device):
-        return pltpu.make_async_remote_copy(
-            src_ref=src, dst_ref=dst, send_sem=send, recv_sem=recv,
-            device_id=device, device_id_type=MESH,
-        )
-
-    chunks = rows // CHUNK
-    first = (rows - HALO) // CHUNK
-    order = list(range(first, chunks)) + list(range(first))
-
-    def x_copy(k, r):
-        part = slice(r * CHUNK, (r + 1) * CHUNK)
-        return remote(
-            x_ref.at[part, :], xw.at[part, aligned(tp, dloc)],
-            xs_sem.at[k - 1, r], xr_sem.at[k - 1, r], (sp, mod(tp + k, tps)),
-        )
-
-    for r in order:
-        for k in range(1, tps):
-            x_copy(k, r).start()
+
     own_x = pltpu.make_async_copy(x_ref, xw.at[:, aligned(tp, dloc)], x_sem)
     own_x.start()
     for p in range(pairs):
@@ -128,6 +107,28 @@
         pltpu.make_async_copy(
             d_ref.at[:, p * LANES : (p + 1) * LANES], d_s.at[p], d_sem
         ).start()
+    pl.semaphore_wait(barrier, len(greeted))
+
+    def remote(src, dst, send, recv, device):
+        return pltpu.make_async_remote_copy(
+            src_ref=src, dst_ref=dst, send_sem=send, recv_sem=recv,
+            device_id=device, device_id_type=MESH,
+        )
+
+    chunks = rows // CHUNK
+    first = (rows - HALO) // CHUNK
+    order = list(range(first, chunks)) + list(range(first))
+
+    def x_copy(k, r):
+        part = slice(r * CHUNK, (r + 1) * CHUNK)
+        return remote(
+            x_ref.at[part, :], xw.at[part, aligned(tp, dloc)],
+            xs_sem.at[k - 1, r], xr_sem.at[k - 1, r], (sp, mod(tp + k, tps)),
+        )
+
+    for r in order:
+        for k in range(1, tps):
+            x_copy(k, r).start()
     own_x.wait()
 
     def turn(t, r):
@@ -140,7 +141,7 @@
 
     zparts = deep // tps
 
-    def share(t, low, high):
+    def share(t, low, high, own):
         for j in range(wide):
             for i in range(2):
                 for q in range(zparts):
@@ -150,13 +151,13 @@
                     cols = pl.ds(pl.multiple_of(mine * rows + low, CHUNK), high - low)
                     dst = xg.at[aligned(zb, feat), cols]
                     if i + j:
-                        remote(src, dst, gs_sem, gr_sem, at(z, y2, c2)).start()
+                        remote(src, dst, gs_sem.at[own], gr_sem.at[own], at(z, y2, c2)).start()
                     else:
-                        pltpu.make_async_copy(src, dst, gl_sem).start()
+                        pltpu.make_async_copy(src, dst, gl_sem.at[own]).start()
 
     for r in range(chunks):
         turn(tp, r)
-    share(tp, 0, rows)
+        share(tp, r * CHUNK, (r + 1) * CHUNK, 0)
 
     pltpu.make_async_copy(wcat, wcat, w_sem).wait()
 
@@ -184,10 +185,27 @@
             ks_sem.at[n], kr_sem.at[n], ahead,
         )
 
+    def cross_copy(k, g):
+        r = order[-1]
+        view = xg.at[
+            aligned(tp, zparts * feat), g * rows + r * CHUNK : g * rows + (r + 1) * CHUNK
+        ]
+        return remote(view, view, gs_sem.at[2], gr_sem.at[2], (sp, mod(tp + k, tps)))
+
+    early = chunks - first - 1
     for n, r in enumerate(order):
         part = slice(r * CHUNK, (r + 1) * CHUNK)
         for k in range(1, tps):
             x_copy(k, r).wait_recv()
+
+        if n == chunks - 1:
+            some = xg.at[: zparts * feat, : (group - 1) * rows]
+            pltpu.make_async_copy(some, some, gr_sem.at[0]).wait()
+            some = xg.at[: zparts * feat, :rows]
+            pltpu.make_async_copy(some, some, gl_sem.at[0]).wait()
+            for k in range(1, tps):
+                for g in range(group):
+                    cross_copy(k, g).start()
 
         @pl.loop(0, pairs)
         def _(p):
@@ -203,16 +221,19 @@
             k_ext[p, HALO + r * CHUNK : HALO + (r + 1) * CHUNK, :] = low[:, LANES : 2 * LANES]
             v_ext[p, HALO + r * CHUNK : HALO + (r + 1) * CHUNK, :] = low[:, 2 * LANES :]
 
-        if n == chunks - first - 1:
+        if n == early:
             @pl.when(has_ahead)
             def _():
                 halo_copy(k_ext, 0).start()
                 halo_copy(v_ext, 1).start()
 
-        for k in range(1, tps):
-            t = mod(tp - k, tps)
-            turn(t, r)
-            share(t, r * CHUNK, (r + 1) * CHUNK)
+        if n < chunks - 1:
+            for k in range(1, tps):
+                t = mod(tp - k, tps)
+                turn(t, r)
+                if n > early:
+                    for done in order[: n + 1] if n == early + 1 else [r]:
+                        share(t, done * CHUNK, (done + 1) * CHUNK, 1)
 
     pltpu.make_async_copy(d_s, d_s, d_sem).wait()
 
@@ -235,6 +256,23 @@
 
     def grad_halo(p):
         return remote(halo_s.at[p], halo_r.at[p], hs_sem.at[p], hr_sem.at[p], behind)
+
+    def to_wide(p, m, k):
+        view = alls[m].at[p, own_rows, :]
+        return remote(
+            view, view, ys_sem.at[m, p, k - 1], yr_sem.at[m, p, k - 1],
+            at(z, mod(y + k, wide), core),
+        )
+
+    def to_mate(p, m, k):
+        owner = aligned(mod(y - k, wide) * 2 + core, rows)
+        view = alls[m].at[p, owner, :]
+        return remote(view, view, cs_sem.at[m, p, k], cr_sem.at[m, p, k], mate)
+
+    def spread_out(p, m):
+        for k in range(1, wide):
+            to_wide(p, m, k).start()
+        to_mate(p, m, 0).start()
 
     def attend(p):
         slot = lax.rem(p, 2)
@@ -273,13 +311,14 @@
             dq_t = jnp.concatenate([dq_t[:HEAD, :QB], dq_t[HEAD:, QB:]], axis=0)
             dq = (dq_t.T * scale).astype(BF)
             xw[part, aligned(p * 3, LANES)] = dq
-            dall[p, pl.ds(pl.multiple_of(mine * rows + block * QB, QB), QB), :LANES] = dq
-        halo_s[p, 0] = kacc[slot, :HALO, :].astype(BF)
-        halo_s[p, 1] = vacc[slot, :HALO, :].astype(BF)
-
-        @pl.when(has_behind)
-        def _():
-            grad_halo(p).start()
+            all_q[p, pl.ds(pl.multiple_of(mine * rows + block * QB, QB), QB), :] = dq
+            if block == HALO // QB - 1:
+                halo_s[p, 0] = kacc[slot, :HALO, :].astype(BF)
+                halo_s[p, 1] = vacc[slot, :HALO, :].astype(BF)
+
+                @pl.when(has_behind)
+                def _():
+                    grad_halo(p).start()
 
         flip_row = lax.broadcasted_iota(jnp.int32, (KB, KB), 0)
         flip_col = lax.broadcasted_iota(jnp.int32, (KB, KB), 1)
@@ -291,17 +330,6 @@
             skewed = pltpu.roll(spread, 0, 1, stride=1, stride_axis=0)
             dline[2 * p + half] = jnp.sum(skewed, axis=0, keepdims=True)
 
-    def to_wide(p, k):
-        view = dall.at[p, own_rows, :]
-        return remote(
-            view, view, ys_sem.at[p, k - 1], yr_sem.at[p, k - 1], at(z, mod(y + k, wide), core)
-        )
-
-    def to_mate(p, k):
-        owner = aligned(mod(y - k, wide) * 2 + core, rows)
-        view = dall.at[p, owner, :]
-        return remote(view, view, cs_sem.at[p, k], cr_sem.at[p, k], mate)
-
     def settle(p):
         slot = lax.rem(p, 2)
 
@@ -314,95 +342,105 @@
         for j, total in ((1, kacc), (2, vacc)):
             low = total[slot, HALO:, :].astype(BF)
             xw[:, aligned(p * 3 + j, LANES)] = low
-            dall[p, own_rows, j * LANES : (j + 1) * LANES] = low
-        for k in range(1, wide):
-            to_wide(p, k).start()
-        to_mate(p, 0).start()
-
-    def forward(p):
-        for k in range(1, wide):
-            to_wide(p, k).wait_recv()
-            to_mate(p, k).start()
+            all_kv[p, own_rows, (j - 1) * LANES : j * LANES] = low
 
     def block_of(b):
         return slice(b * feat, (b + 1) * feat)
 
-    def to_right(p, b):
+    def to_right(p, m, b):
+        view = rights[m].at[p, b]
+        return remote(view, view, rs_sem.at[m, p, b], rv_sem.at[m, p, b], at(z + 1, y, core))
+
+    def to_left(p, m, b):
+        view = lefts[m].at[p, b]
+        return remote(view, view, ls_sem.at[m, p, b], lv_sem.at[m, p, b], at(z - 1, y, core))
+
+    def hop(p, m, h):
+        @pl.when(z == h)
+        def _():
+            for b in range(deep - 1, h, -1):
+                total = zacc[p, block_of(b), lanes[m]]
+                if h:
+                    to_right(p, m, b).wait_recv()
+                    total = total + rights[m][p, b].astype(F32)
+                rights[m][p, b] = total.astype(BF)
+                to_right(p, m, b).start()
+
+        @pl.when(z == deep - 1 - h)
+        def _():
+            for b in range(0, deep - 1 - h):
+                total = zacc[p, block_of(b), lanes[m]]
+                if h:
+                    to_left(p, m, b).wait_recv()
+                    total = total + lefts[m][p, b].astype(F32)
+                lefts[m][p, b] = total.astype(BF)
+                to_left(p, m, b).start()
+
+    def forward(p, m):
+        for k in range(1, wide):
+            to_wide(p, m, k).wait_recv()
+            to_mate(p, m, k).start()
+
+    def product(p, m):
+        if m == 0:
+            @pl.when(p == 0)
+            def _():
+                others = slice(0, (deep - zparts) * feat)
+                some = xg.at[others, : (group - 1) * (rows - CHUNK)]
+                pltpu.make_async_copy(some, some, gr_sem.at[1]).wait()
+                some = xg.at[others, : rows - CHUNK]
+                pltpu.make_async_copy(some, some, gl_sem.at[1]).wait()
+                some = xg.at[others, : group * CHUNK]
+                pltpu.make_async_copy(some, some, gr_sem.at[2]).wait()
+
+        for k in range(wide):
+            to_mate(p, m, k).wait_recv()
+        zacc[p, : deep * feat, lanes[m]] = dot32(xg[...], alls[m][p], ((1,), (0,)))
+        hop(p, m, 0)
+
+    def finish(p, m):
+        me = aligned(z, feat)
+
+        @pl.when(z > 0)
+        def _():
+            to_right(p, m, z).wait_recv()
+            zacc[p, me, lanes[m]] += rights[m][p, z].astype(F32)
+
+        @pl.when(z < deep - 1)
+        def _():
+            to_left(p, m, z).wait_recv()
+            zacc[p, me, lanes[m]] += lefts[m][p, z].astype(F32)
+
+        total = zacc[p, me, lanes[m]]
+        for j, ref in enumerate((dwk_ref, dwv_ref) if m else (dwq_ref,)):
+            ref[:, aligned(p, LANES)] = total[:, j * LANES : (j + 1) * LANES]
+
+    def near_copy(j, i):
+        view = near.at[mine]
         return remote(
-            rr.at[p, b], rr.at[p, b], rs_sem.at[p, b], rv_sem.at[p, b], at(z + 1, y, core)
-        )
-
-    def to_left(p, b):
-        return remote(
-            rl.at[p, b], rl.at[p, b], ls_sem.at[p, b], lv_sem.at[p, b], at(z - 1, y, core)
-        )
-
-    def hop(p, h):
-        @pl.when(z == h)
-        def _():
-            for b in range(deep - 1, h, -1):
-                total = zacc[p, block_of(b), :]
-                if h:
-                    to_right(p, b).wait_recv()
-                    total = total + rr[p, b].astype(F32)
-                rr[p, b] = total.astype(BF)
-                to_right(p, b).start()
-
-        @pl.when(z == deep - 1 - h)
-        def _():
-            for b in range(0, deep - 1 - h):
-                total = zacc[p, block_of(b), :]
-                if h:
-                    to_left(p, b).wait_recv()
-                    total = total + rl[p, b].astype(F32)
-                rl[p, b] = total.astype(BF)
-                to_left(p, b).start()
-
-    def product(p):
-        for k in range(wide):
-            to_mate(p, k).wait_recv()
-
-        @pl.when(p == 0)
-        def _():
-            some = xg.at[:, : (group - 1) * rows]
-            pltpu.make_async_copy(some, some, gr_sem).wait()
-            some = xg.at[:, :rows]
-            pltpu.make_async_copy(some, some, gl_sem).wait()
-
-        zacc[p, : deep * feat, :] = dot32(xg[...], dall[p], ((1,), (0,)))
-        hop(p, 0)
-
-    def finish(p):
-        me = aligned(z, feat)
-
-        @pl.when(z > 0)
-        def _():
-            to_right(p, z).wait_recv()
-            zacc[p, me, :] += rr[p, z].astype(F32)
-
-        @pl.when(z < deep - 1)
-        def _():
-            to_left(p, z).wait_recv()
-            zacc[p, me, :] += rl[p, z].astype(F32)
-
-        total = zacc[p, me, :]
-        for j, ref in enumerate((dwq_ref, dwk_ref, dwv_ref)):
-            ref[:, aligned(p, LANES)] = total[:, j * LANES : (j + 1) * LANES]
-
-    def bias_copy(k):
-        return remote(
-            bslot.at[k], brecv.at[k], bs_sem.at[k], br_sem.at[k],
-            (jnp.bitwise_xor(sp, 1 << k), tp),
-        )
-
-    def bias_step(k):
-        if k:
-            bias_copy(k - 1).wait_recv()
-            bslot[k] = bslot[k - 1] + brecv[k - 1]
-        else:
-            bslot[0] = jnp.concatenate([dline[n] for n in range(2 * pairs)], axis=0)
-        if k < steps:
-            bias_copy(k).start()
+            view, view, bs_sem.at[0], br_sem.at[0], at(z, mod(y + j, wide), mod(core + i, 2))
+        )
+
+    def far_copy(k):
+        view = far.at[z]
+        return remote(view, view, bs_sem.at[1], br_sem.at[1], at(mod(z + k, deep), y, core))
+
+    mates = [(j, i) for j in range(wide) for i in range(2) if i + j]
+
+    def bias_near():
+        near[mine] = jnp.concatenate([dline[n] for n in range(2 * pairs)], axis=0)
+        for j, i in mates:
+            near_copy(j, i).start()
+
+    def bias_far():
+        some = near.at[: group - 1]
+        pltpu.make_async_copy(some, some, br_sem.at[0]).wait()
+        total = near[0]
+        for n in range(1, group):
+            total = total + near[n]
+        far[z] = total
+        for k in range(1, deep):
+            far_copy(k).start()
 
     tiles = dloc // TILE
     away = (tps - 1) * tiles
@@ -428,10 +466,10 @@
             gi_ref[:, aligned(j - away, TILE)] = low
 
     hops = deep - 2
-    lag_end = 5 + hops
-    rounds = pairs + lag_end + 1
-    late = rounds - (pairs + 1)
-    per = -(-tps * tiles // late)
+    ready = pairs // 2
+    last = 1 + 2 * (hops + 1)
+    rounds = 3 * pairs - ready + last
+    per = 2
 
     def staged(i, lag, stage):
         p = i - lag
@@ -439,35 +477,67 @@
         @pl.when((p >= 0) & (p < pairs))
         def _():
             stage(p)
+
+    def pieced(i, lag, stage):
+        n = i - lag
+        odd = lax.rem(n + 2 * last, 2) == 1
+        before = jnp.where(odd & (n > 0), lax.div(n - 1, 2), -1)
+        piece = jnp.where(n < pairs, before, n - pairs + ready)
+        for m in range(2):
+            @pl.when((piece >= 0) & (piece < 2 * pairs) & (lax.rem(piece + 2, 2) == m))
+            def _():
+                stage(lax.div(piece, 2), m)
 
     @pl.loop(0, rounds)
     def _(i):
         staged(i, 0, attend)
+
+        @pl.when(i == pairs - 1)
+        def _():
+            bias_near()
+
         staged(i, 1, settle)
-        staged(i, 3, forward)
-        staged(i, 4, product)
+        for m in range(2):
+            @pl.when((i < pairs) & (lax.rem(i, 3) == m))
+            def _():
+                spread_out(lax.div(i, 3), m)
+
+        @pl.when(i == pairs)
+        def _():
+            for p in range(pairs):
+                for m in range(2):
+                    if 3 * p + m >= pairs:
+                        spread_out(p, m)
+
+        pieced(i, 1, product)
         for h in range(1, hops + 1):
-            staged(i, 4 + h, functools.partial(hop, h=h))
-        staged(i, lag_end, finish)
-        for k in range(steps + 1):
-            @pl.when(i == pairs + k)
-            def _():
-                bias_step(k)
-
-        @pl.when(i > pairs)
+            pieced(i, 1 + 2 * h, functools.partial(hop, h=h))
+        pieced(i, last, finish)
+        pieced(i, 0, forward)
+
+        @pl.when(i == pairs + 3)
+        def _():
+            bias_far()
+
+        @pl.when(i >= pairs)
         def _():
             @pl.loop(0, per)
             def _(n):
-                j = (i - pairs - 1) * per + n
+                j = (i - pairs) * per + n
 
                 @pl.when(j < tps * tiles)
                 def _():
                     input_tile(j)
 
+    some = far.at[: deep - 1]
+    pltpu.make_async_copy(some, some, br_sem.at[1]).wait()
+    summed = far[0]
+    for n in range(1, deep):
+        summed = summed + far[n]
     spot = lax.broadcasted_iota(jnp.int32, (rel_ref.shape[1], LINE), 1)
     back = bias_index(spot - (KB - 1))
     entry = lax.broadcasted_iota(jnp.int32, (rel_ref.shape[1], LINE), 0)
-    gb_ref[...] = exact(bslot[steps], jnp.where(back == entry, 1.0, 0.0), ((1,), (1,)))
+    gb_ref[...] = exact(summed, jnp.where(back == entry, 1.0, 0.0), ((1,), (1,)))
 
     pltpu.make_async_copy(pxr, pxr, pr_sem).wait()
     for n in range(tiles):
@@ -481,16 +551,22 @@
     for r in order:
         for k in range(1, tps):
             x_copy(k, r).wait_send()
-    some = xg.at[:, : (group - 1) * rows]
-    pltpu.make_async_copy(some, some, gs_sem).wait()
+    some = xg.at[: zparts * feat, : (group - 1) * rows]
+    pltpu.make_async_copy(some, some, gs_sem.at[0]).wait()
+    some = xg.at[: (deep - zparts) * feat, : (group - 1) * (rows - CHUNK)]
+    pltpu.make_async_copy(some, some, gs_sem.at[1]).wait()
+    some = xg.at[: (deep - zparts) * feat, : group * CHUNK]
+    pltpu.make_async_copy(some, some, gs_sem.at[2]).wait()
 
     @pl.when(has_ahead)
     def _():
         halo_copy(k_ext, 0).wait_send()
         halo_copy(v_ext, 1).wait_send()
 
-    for k in range(steps):
-        bias_copy(k).wait_send()
+    for j, i in mates:
+        near_copy(j, i).wait_send()
+    for k in range(1, deep):
+        far_copy(k).wait_send()
 
     @pl.loop(0, pairs)
     def _(p):
@@ -498,18 +574,19 @@
         def _():
             grad_halo(p).wait_send()
 
-        for k in range(1, wide):
-            to_wide(p, k).wait_send()
-        for k in range(wide):
-            to_mate(p, k).wait_send()
-        for b in range(deep):
-            @pl.when(z < b)
-            def _():
-                to_right(p, b).wait_send()
-
-            @pl.when(z > b)
-            def _():
-                to_left(p, b).wait_send()
+        for m in range(2):
+            for k in range(1, wide):
+                to_wide(p, m, k).wait_send()
+            for k in range(wide):
+                to_mate(p, m, k).wait_send()
+            for b in range(deep):
+                @pl.when(z < b)
+                def _():
+                    to_right(p, m, b).wait_send()
+
+                @pl.when(z > b)
+                def _():
+                    to_left(p, m, b).wait_send()
 
 
 def local(sizes, inputs, w_query, w_key, w_value, rel_bias, d_out):
@@ -522,7 +599,6 @@
     feat = full // seq
     group = 2 * wide
     tiles = dloc // TILE
-    steps = seq.bit_length() - 1
     chunks = rows // CHUNK
     heads = rel_bias.shape[1]
     sds = jax.ShapeDtypeStruct
@@ -557,23 +633,26 @@
             vm((2, ext, LANES), F32),
             vm((pairs, 2, HALO, LANES), BF),
             vm((pairs, 2, HALO, LANES), BF),
-            vm((pairs, group * rows, TRIO), BF),
-            vm((pairs, deep, feat, TRIO), BF),
-            vm((pairs, deep, feat, TRIO), BF),
+            vm((pairs, group * rows, LANES), BF),
+            vm((pairs, group * rows, 2 * LANES), BF),
+            vm((pairs, deep, feat, LANES), BF),
+            vm((pairs, deep, feat, 2 * LANES), BF),
+            vm((pairs, deep, feat, LANES), BF),
+            vm((pairs, deep, feat, 2 * LANES), BF),
             vm(((tps - 1) * tiles, rows, TILE), BF),
             vm(((tps - 1) * tiles, rows, TILE), BF),
-            vm((steps + 1, 2 * pairs, LINE), F32),
-            vm((steps, 2 * pairs, LINE), F32),
+            vm((group, 2 * pairs, LINE), F32),
+            vm((deep, 2 * pairs, LINE), F32),
             dma(()), dma(()), dma(()),
             dma((tps - 1, chunks)), dma((tps - 1, chunks)),
-            dma(()), dma(()), dma(()),
+            dma((3,)), dma((3,)), dma((2,)),
             dma((2,)), dma((2,)),
             dma((pairs,)), dma((pairs,)),
-            dma((pairs, wide - 1)), dma((pairs, wide - 1)),
-            dma((pairs, wide)), dma((pairs, wide)),
-            dma((pairs, deep)), dma((pairs, deep)),
-            dma((pairs, deep)), dma((pairs, deep)),
-            dma((steps,)), dma((steps,)),
+            dma((2, pairs, wide - 1)), dma((2, pairs, wide - 1)),
+            dma((2, pairs, wide)), dma((2, pairs, wide)),
+            dma((2, pairs, deep)), dma((2, pairs, deep)),
+            dma((2, pairs, deep)), dma((2, pairs, deep)),
+            dma((2,)), dma((2,)),
             dma(()), dma(()),
         ],
         compiler_params=pltpu.CompilerParams(

time: 171 us -> 149 us (0.87)
  Pallas kernels: 163 us -> 141 us
    pallas_call x1, Pallas kernels: 163 us -> 141 us  [local(): pl.pallas_call(functools.partial(step_body, sizes), in_specs=[hbm, hbm, h...]
where the time goes in v2:
time: 149 us
  Pallas kernels  141 us (95%)
  local copies, waits for them, and re-layouts  6.91 us (5%)
    pallas_call x1, Pallas kernels, local(): pl.pallas_call(functools.partial(step_body, sizes), in_specs=[hbm, hbm, h...  141 us
    unnamed x11, local copies, waits for them, and re-layouts  6.91 us

profile of v2, /device:TPU:0, one launch (start us, length us, event | category | flops | bytes accessed | tf_op | source)
XLA Modules:
  0.0 149.0 jit_solution(111468243966012317)
XLA Ops:
  0.6 141.4 %whole_step.1 = (bf16[512,1536]{1,0:T(8,128)(2,1)}, f32[192,768]{1,0:T(8,128)}, f32[192,768]{1,0:T(8,128)}, f32[192,768]{1,0:T(8,128)}, f32[12,320]{1,0:T(8,128)}) custom-call(bf16[512,1536]{1,0:T(8,128)(2,1)} %x_ref.1, bf16[3072,768]{1,0:T(8,128)(2,1)} %wq_ref.1, bf16[3072,768]{1,0:T(8,128)(2,1)} %wk_ref.1, bf16[3072,768]{1,0:T(8,128)(2,1)} %wv_ref.1, ...), custom_call_target="tpu_custom_call" | custom-call | tf_op jit(solution)/shard_map/whole_step/pallas_call | solution.py:609
  142.0 0.0 copy-start.1
  142.0 0.0 copy-start
  142.1 0.0 copy-start.2
  142.1 2.7 %copy.16 = bf16[512,1536]{1,0:T(8,128)(2,1)} copy(bf16[512,1536]{1,0:T(8,128)(2,1)} %get-tuple-element.20) | data formatting | bytes 3145728
  144.8 1.9 %copy.17 = f32[192,768]{1,0:T(8,128)} copy(f32[192,768]{1,0:T(8,128)} %get-tuple-element.21) | data formatting | bytes 1179648
  146.7 0.0 copy-done.1
  146.7 0.8 copy.18
  147.5 0.0 copy-done
  147.6 0.8 copy.19
  148.4 0.0 copy-done.2
  148.4 0.6 copy.20
Async XLA Ops:
  142.0 4.7 %copy-start.1 = (f32[192,768]{1,0:T(8,128)S(1)}, f32[192,768]{1,0:T(8,128)}, u32[]{:S(2)}) copy-start(f32[192,768]{1,0:T(8,128)} %get-tuple-element.22) | copy-start | bytes 1769476
  142.0 5.5 %copy-start = (f32[192,768]{1,0:T(8,128)S(1)}, f32[192,768]{1,0:T(8,128)}, u32[]{:S(2)}) copy-start(f32[192,768]{1,0:T(8,128)} %get-tuple-element.23) | copy-start | bytes 1769476
  142.1 6.3 %copy-start.2 = (f32[12,320]{1,0:T(8,128)S(1)}, f32[12,320]{1,0:T(8,128)}, u32[]{:S(2)}) copy-start(f32[12,320]{1,0:T(8,128)} %get-tuple-element.14) | copy-start | bytes 46084

commit v3 on v2

--- a/solution.py
+++ b/solution.py
@@ -53,9 +53,10 @@
 def step_body(
     sizes,
     x_ref, wq_ref, wk_ref, wv_ref, rel_ref, d_ref,
-    gi_ref, dwq_ref, dwk_ref, dwv_ref, gb_ref,
+    gi_out, dw_out, gb_out,
     xw, wcat, xt, xg, zacc, q_s, k_ext, v_ext, d_s, lines, dline, bias, bias_sum, kacc, vacc,
     halo_s, halo_r, all_q, all_kv, right_q, right_kv, left_q, left_kv, pxs, pxr, near, far,
+    xl, gi_ref, dw_ref, gb_ref, o_sem,
     w_sem, d_sem, x_sem, xs_sem, xr_sem, gs_sem, gr_sem, gl_sem, ks_sem, kr_sem, hs_sem, hr_sem,
     ys_sem, yr_sem, cs_sem, cr_sem, rs_sem, rv_sem, ls_sem, lv_sem, bs_sem, br_sem, ps_sem, pr_sem,
 ):
@@ -121,8 +122,9 @@
 
     def x_copy(k, r):
         part = slice(r * CHUNK, (r + 1) * CHUNK)
+        landing = xl.at[k - 1] if r == order[-1] else xw.at[part, aligned(tp, dloc)]
         return remote(
-            x_ref.at[part, :], xw.at[part, aligned(tp, dloc)],
+            x_ref.at[part, :], landing,
             xs_sem.at[k - 1, r], xr_sem.at[k - 1, r], (sp, mod(tp + k, tps)),
         )
 
@@ -131,17 +133,20 @@
             x_copy(k, r).start()
     own_x.wait()
 
-    def turn(t, r):
+    def turn(t, r, source=None):
         part = slice(r * CHUNK, (r + 1) * CHUNK)
 
         @pl.loop(0, dloc // TILE)
         def _(f):
             cols = aligned(t * (dloc // TILE) + f, TILE)
-            xt[cols, part] = xw[part, cols].T
+            if source is None:
+                xt[cols, part] = xw[part, cols].T
+            else:
+                xt[cols, part] = xl[source, :, aligned(f, TILE)].T
 
     zparts = deep // tps
 
-    def share(t, low, high, own):
+    def share(t, low, high, own, afar=True):
         for j in range(wide):
             for i in range(2):
                 for q in range(zparts):
@@ -150,6 +155,8 @@
                     src = xt.at[aligned((zb * wide + y2) * 2 + c2, feat), low:high]
                     cols = pl.ds(pl.multiple_of(mine * rows + low, CHUNK), high - low)
                     dst = xg.at[aligned(zb, feat), cols]
+                    if i + j and not afar:
+                        continue
                     if i + j:
                         remote(src, dst, gs_sem.at[own], gr_sem.at[own], at(z, y2, c2)).start()
                     else:
@@ -186,15 +193,26 @@
         )
 
     def cross_copy(k, g):
-        r = order[-1]
-        view = xg.at[
-            aligned(tp, zparts * feat), g * rows + r * CHUNK : g * rows + (r + 1) * CHUNK
-        ]
+        cols = pl.ds(pl.multiple_of(mod(mine + g, group) * rows, rows), rows - HALO)
+        view = xg.at[aligned(tp, zparts * feat), cols]
         return remote(view, view, gs_sem.at[2], gr_sem.at[2], (sp, mod(tp + k, tps)))
+
+    def project(p, r):
+        part = slice(r * CHUNK, (r + 1) * CHUNK)
+        total = zacc[p, part, :]
+        for k in range(1, tps):
+            t = mod(tp - k, tps)
+            whole = xl[k - 1] if r == order[-1] else xw[part, aligned(t, dloc)]
+            total = total + dot32(
+                whole, wcat[aligned(t, dloc), aligned(p, TRIO)], ((1,), (0,))
+            )
+        low = total.astype(BF)
+        q_s[p, part, :] = low[:, :LANES]
+        k_ext[p, HALO + r * CHUNK : HALO + (r + 1) * CHUNK, :] = low[:, LANES : 2 * LANES]
+        v_ext[p, HALO + r * CHUNK : HALO + (r + 1) * CHUNK, :] = low[:, 2 * LANES :]
 
     early = chunks - first - 1
     for n, r in enumerate(order):
-        part = slice(r * CHUNK, (r + 1) * CHUNK)
         for k in range(1, tps):
             x_copy(k, r).wait_recv()
 
@@ -204,22 +222,13 @@
             some = xg.at[: zparts * feat, :rows]
             pltpu.make_async_copy(some, some, gl_sem.at[0]).wait()
             for k in range(1, tps):
-                for g in range(group):
+                for g in range(1, group):
                     cross_copy(k, g).start()
 
-        @pl.loop(0, pairs)
-        def _(p):
-            total = zacc[p, part, :]
-            for k in range(1, tps):
-                t = mod(tp - k, tps)
-                total = total + dot32(
-                    xw[part, aligned(t, dloc)], wcat[aligned(t, dloc), aligned(p, TRIO)],
-                    ((1,), (0,)),
-                )
-            low = total.astype(BF)
-            q_s[p, part, :] = low[:, :LANES]
-            k_ext[p, HALO + r * CHUNK : HALO + (r + 1) * CHUNK, :] = low[:, LANES : 2 * LANES]
-            v_ext[p, HALO + r * CHUNK : HALO + (r + 1) * CHUNK, :] = low[:, 2 * LANES :]
+        if n < chunks - 1:
+            @pl.loop(0, pairs)
+            def _(p):
+                project(p, r)
 
         if n == early:
             @pl.when(has_ahead)
@@ -227,13 +236,15 @@
                 halo_copy(k_ext, 0).start()
                 halo_copy(v_ext, 1).start()
 
-        if n < chunks - 1:
-            for k in range(1, tps):
-                t = mod(tp - k, tps)
+        for k in range(1, tps):
+            t = mod(tp - k, tps)
+            if n < chunks - 1:
                 turn(t, r)
-                if n > early:
-                    for done in order[: n + 1] if n == early + 1 else [r]:
-                        share(t, done * CHUNK, (done + 1) * CHUNK, 1)
+            if n == min(early + 1, chunks - 1):
+                for done in order[: early + 1]:
+                    share(t, done * CHUNK, (done + 1) * CHUNK, 1)
+            if early < n < chunks - 1:
+                share(t, r * CHUNK, (r + 1) * CHUNK, 1, afar=False)
 
     pltpu.make_async_copy(d_s, d_s, d_sem).wait()
 
@@ -275,6 +286,7 @@
         to_mate(p, m, 0).start()
 
     def attend(p):
+        project(p, order[-1])
         slot = lax.rem(p, 2)
         offset = key_row - jnp.where(query_row < SEG, 0, SEG)
         seen = (offset >= 0) & (offset < HALO + SEG)
@@ -386,11 +398,11 @@
             @pl.when(p == 0)
             def _():
                 others = slice(0, (deep - zparts) * feat)
-                some = xg.at[others, : (group - 1) * (rows - CHUNK)]
+                some = xg.at[others, : (group - 1) * HALO]
                 pltpu.make_async_copy(some, some, gr_sem.at[1]).wait()
-                some = xg.at[others, : rows - CHUNK]
+                some = xg.at[others, :rows]
                 pltpu.make_async_copy(some, some, gl_sem.at[1]).wait()
-                some = xg.at[others, : group * CHUNK]
+                some = xg.at[others, : (group - 1) * (rows - HALO)]
                 pltpu.make_async_copy(some, some, gr_sem.at[2]).wait()
 
         for k in range(wide):
@@ -398,6 +410,10 @@
         zacc[p, : deep * feat, lanes[m]] = dot32(xg[...], alls[m][p], ((1,), (0,)))
         hop(p, m, 0)
 
+    def grad_out(p, j):
+        cols = aligned(p, LANES)
+        return pltpu.make_async_copy(dw_ref.at[j, :, cols], dw_out.at[j, :, cols], o_sem.at[0])
+
     def finish(p, m):
         me = aligned(z, feat)
 
@@ -412,8 +428,9 @@
             zacc[p, me, lanes[m]] += lefts[m][p, z].astype(F32)
 
         total = zacc[p, me, lanes[m]]
-        for j, ref in enumerate((dwk_ref, dwv_ref) if m else (dwq_ref,)):
-            ref[:, aligned(p, LANES)] = total[:, j * LANES : (j + 1) * LANES]
+        for j in range(1 + m):
+            dw_ref[m + j, :, aligned(p, LANES)] = total[:, j * LANES : (j + 1) * LANES]
+            grad_out(p, m + j).start()
 
     def near_copy(j, i):
         view = near.at[mine]
@@ -466,9 +483,9 @@
             gi_ref[:, aligned(j - away, TILE)] = low
 
     hops = deep - 2
-    ready = pairs // 2
-    last = 1 + 2 * (hops + 1)
-    rounds = 3 * pairs - ready + last
+    early_pieces = pairs - 1
+    last = 3 + 2 * (hops + 1)
+    rounds = 2 * pairs + last
     per = 2
 
     def staged(i, lag, stage):
@@ -479,14 +496,18 @@
             stage(p)
 
     def pieced(i, lag, stage):
-        n = i - lag
-        odd = lax.rem(n + 2 * last, 2) == 1
-        before = jnp.where(odd & (n > 0), lax.div(n - 1, 2), -1)
-        piece = jnp.where(n < pairs, before, n - pairs + ready)
+        piece = i - lag
+        valid = (piece >= 0) & (piece < 2 * pairs)
+        mixed = piece < early_pieces
+        kv_left = pairs - early_pieces // 2
+        parity = lax.rem(piece + 2 * last, 2)
+        is_kv = jnp.where(mixed, parity, jnp.where(piece < early_pieces + kv_left, 1, 0))
+        late_pair = jnp.where(is_kv == 1, piece - early_pieces + early_pieces // 2, piece - pairs)
+        pair = jnp.where(mixed, lax.div(piece, 2), late_pair)
         for m in range(2):
-            @pl.when((piece >= 0) & (piece < 2 * pairs) & (lax.rem(piece + 2, 2) == m))
+            @pl.when(valid & (is_kv == m))
             def _():
-                stage(lax.div(piece, 2), m)
+                stage(pair, m)
 
     @pl.loop(0, rounds)
     def _(i):
@@ -498,22 +519,29 @@
 
         staged(i, 1, settle)
         for m in range(2):
-            @pl.when((i < pairs) & (lax.rem(i, 3) == m))
+            @pl.when((i < early_pieces) & (lax.rem(i, 2) == m))
             def _():
-                spread_out(lax.div(i, 3), m)
+                spread_out(lax.div(i, 2), m)
+
+        @pl.when(i == 0)
+        def _():
+            for k in range(1, tps):
+                r = order[-1]
+                turn(mod(tp - k, tps), r, k - 1)
+                share(mod(tp - k, tps), r * CHUNK, (r + 1) * CHUNK, 1, afar=False)
 
         @pl.when(i == pairs)
         def _():
-            for p in range(pairs):
-                for m in range(2):
-                    if 3 * p + m >= pairs:
+            for m in (1, 0):
+                for p in range(pairs):
+                    if 2 * p + m >= early_pieces:
                         spread_out(p, m)
 
-        pieced(i, 1, product)
+        pieced(i, 3, product)
         for h in range(1, hops + 1):
-            pieced(i, 1 + 2 * h, functools.partial(hop, h=h))
+            pieced(i, 3 + 2 * h, functools.partial(hop, h=h))
         pieced(i, last, finish)
-        pieced(i, 0, forward)
+        pieced(i, 2, forward)
 
         @pl.when(i == pairs + 3)
         def _():
@@ -539,6 +567,7 @@
     entry = lax.broadcasted_iota(jnp.int32, (rel_ref.shape[1], LINE), 0)
     gb_ref[...] = exact(summed, jnp.where(back == entry, 1.0, 0.0), ((1,), (1,)))
 
+    pltpu.make_async_copy(gb_ref, gb_out, o_sem.at[2]).start()
     pltpu.make_async_copy(pxr, pxr, pr_sem).wait()
     for n in range(tiles):
         cols = slice(n * TILE, (n + 1) * TILE)
@@ -546,6 +575,7 @@
         for k in range(1, tps):
             total = total + pxr[(k - 1) * tiles + n].astype(F32)
         gi_ref[:, cols] = total.astype(BF)
+        pltpu.make_async_copy(gi_ref.at[:, cols], gi_out.at[:, cols], o_sem.at[1]).start()
 
     pltpu.make_async_copy(pxs, pxs, ps_sem).wait()
     for r in order:
@@ -553,9 +583,9 @@
             x_copy(k, r).wait_send()
     some = xg.at[: zparts * feat, : (group - 1) * rows]
     pltpu.make_async_copy(some, some, gs_sem.at[0]).wait()
-    some = xg.at[: (deep - zparts) * feat, : (group - 1) * (rows - CHUNK)]
+    some = xg.at[: (deep - zparts) * feat, : (group - 1) * HALO]
     pltpu.make_async_copy(some, some, gs_sem.at[1]).wait()
-    some = xg.at[: (deep - zparts) * feat, : group * CHUNK]
+    some = xg.at[: (deep - zparts) * feat, : (group - 1) * (rows - HALO)]
     pltpu.make_async_copy(some, some, gs_sem.at[2]).wait()
 
     @pl.when(has_ahead)
@@ -587,6 +617,26 @@
                 @pl.when(z > b)
                 def _():
                     to_left(p, m, b).wait_send()
+
+    pltpu.make_async_copy(dw_ref, dw_out, o_sem.at[0]).wait()
+    pltpu.make_async_copy(gi_ref, gi_out, o_sem.at[1]).wait()
+    pltpu.make_async_copy(gb_ref, gb_out, o_sem.at[2]).wait()
+
+
+def hand_body(gi, dw, gb, gi_out, dwq_out, dwk_out, dwv_out, gb_out, gi_v, dw_v, gb_v, i_sem, o_sem):
+    outs = (dwq_out, dwk_out, dwv_out)
+    rows = gi.shape[0] // 2
+    moves = [(gi.at[n * rows : (n + 1) * rows], gi_v.at[n * rows : (n + 1) * rows],
+              gi_out.at[n * rows : (n + 1) * rows]) for n in range(2)]
+    moves += [(dw.at[j], dw_v.at[j], outs[j]) for j in range(3)]
+    moves.append((gb, gb_v, gb_out))
+    for n, (src, mid, _) in enumerate(moves):
+        pltpu.make_async_copy(src, mid, i_sem.at[n]).start()
+    for n, (src, mid, dst) in enumerate(moves):
+        pltpu.make_async_copy(src, mid, i_sem.at[n]).wait()
+        pltpu.make_async_copy(mid, dst, o_sem.at[n]).start()
+    for n, (_, mid, dst) in enumerate(moves):
+        pltpu.make_async_copy(mid, dst, o_sem.at[n]).wait()
 
 
 def local(sizes, inputs, w_query, w_key, w_value, rel_bias, d_out):
@@ -609,10 +659,10 @@
     out = pl.pallas_call(
         functools.partial(step_body, sizes),
         in_specs=[hbm, hbm, hbm, hbm, on_chip, hbm],
-        out_specs=[on_chip] * 5,
+        out_specs=[hbm] * 3,
         out_shape=[
             sds((rows, dloc), BF),
-            sds((feat, width), F32), sds((feat, width), F32), sds((feat, width), F32),
+            sds((3, feat, width), F32),
             sds((heads, rel_bias.shape[0]), F32),
         ],
         scratch_shapes=[
@@ -643,6 +693,11 @@
             vm(((tps - 1) * tiles, rows, TILE), BF),
             vm((group, 2 * pairs, LINE), F32),
             vm((deep, 2 * pairs, LINE), F32),
+            vm((tps - 1, CHUNK, dloc), BF),
+            vm((rows, dloc), BF),
+            vm((3, feat, width), F32),
+            vm((heads, rel_bias.shape[0]), F32),
+            dma((3,)),
             dma(()), dma(()), dma(()),
             dma((tps - 1, chunks)), dma((tps - 1, chunks)),
             dma((3,)), dma((3,)), dma((2,)),
@@ -660,6 +715,18 @@
         ),
         name="whole_step",
     )(inputs, w_query, w_key, w_value, rel_bias.T, d_out)
+    grad = sds((feat, width), F32)
+    out = pl.pallas_call(
+        hand_body,
+        in_specs=[hbm] * 3,
+        out_specs=[hbm] * 5,
+        out_shape=[sds((rows, dloc), BF), grad, grad, grad, sds((heads, rel_bias.shape[0]), F32)],
+        scratch_shapes=[
+            vm((rows, dloc), BF), vm((3, feat, width), F32), vm((heads, rel_bias.shape[0]), F32),
+            dma((6,)), dma((6,)),
+        ],
+        name="hand_out",
+    )(*out)
     return out[0], out[1], out[2], out[3], out[4].T
 
 

time: 149 us -> 140 us (0.940)
  local copies, waits for them, and re-layouts: 6.91 us -> 0 us
  Pallas kernels: 141 us -> 139 us
    unnamed x11 -> x0, local copies, waits for them, and re-layouts: 6.91 us -> none
    pallas_call x1, Pallas kernels: 141 us -> 136 us  [local(): pl.pallas_call(functools.partial(step_body, sizes), in_specs=[hbm, hbm, h...]
    pallas_call x0 -> x1, Pallas kernels: none -> 2.96 us  [local(): pl.pallas_call(hand_body, in_specs=[hbm] * 3, out_specs=[hbm] * 5, out_sh...]
where the time goes in v3:
time: 140 us
  Pallas kernels  139 us (99%)
    pallas_call x1, Pallas kernels, local(): pl.pallas_call(functools.partial(step_body, sizes), in_specs=[hbm, hbm, h...  136 us
    pallas_call x1, Pallas kernels, local(): pl.pallas_call(hand_body, in_specs=[hbm] * 3, out_specs=[hbm] * 5, out_sh...  2.96 us

profile of v3, /device:TPU:0, one launch (start us, length us, event | category | flops | bytes accessed | tf_op | source)
XLA Modules:
  0.0 140.0 jit_solution(4048539760218899110)
XLA Ops:
  0.6 136.4 %whole_step.1 = (bf16[512,1536]{1,0:T(8,128)(2,1)}, f32[3,192,768]{2,1,0:T(8,128)}, f32[12,320]{1,0:T(8,128)}) custom-call(bf16[512,1536]{1,0:T(8,128)(2,1)} %x_ref.1, bf16[3072,768]{1,0:T(8,128)(2,1)} %wq_ref.1, bf16[3072,768]{1,0:T(8,128)(2,1)} %wk_ref.1, bf16[3072,768]{1,0:T(8,128)(2,1)} %wv_ref.1, f32[12,320]{1,0:T(8,128)} %bitcast.2, bf16[512,768]{1,0:T(8,128)(2,1)} %d_ref.1), custom_call_target="tpu_custom_call" | custom-call | tf_op jit(solution)/shard_map/whole_step/pallas_call | solution.py:659
  137.0 3.0 %hand_out.1 = (bf16[512,1536]{1,0:T(8,128)(2,1)}, f32[192,768]{1,0:T(8,128)}, f32[192,768]{1,0:T(8,128)}, f32[192,768]{1,0:T(8,128)}, f32[12,320]{1,0:T(8,128)}) custom-call(bf16[512,1536]{1,0:T(8,128)(2,1)} %get-tuple-element.13.gi, f32[3,192,768]{2,1,0:T(8,128)} %get-tuple-element.14.dw, f32[12,320]{1,0:T(8,128)} %get-tuple-element.15.gb), custom_call_target="tpu_custom_call" | custom-call | tf_op jit(solution)/shard_map/hand_out/pallas_call | solution.py:719

commit v4 on v3

--- a/solution.py
+++ b/solution.py
@@ -266,26 +266,26 @@
         )
 
     def grad_halo(p):
-        return remote(halo_s.at[p], halo_r.at[p], hs_sem.at[p], hr_sem.at[p], behind)
+        return remote(halo_s.at[p], halo_r.at[p], hs_sem, hr_sem.at[p], behind)
 
     def to_wide(p, m, k):
         view = alls[m].at[p, own_rows, :]
         return remote(
-            view, view, ys_sem.at[m, p, k - 1], yr_sem.at[m, p, k - 1],
+            view, view, ys_sem.at[m, k - 1], yr_sem.at[m, p, k - 1],
             at(z, mod(y + k, wide), core),
         )
 
     def to_mate(p, m, k):
         owner = aligned(mod(y - k, wide) * 2 + core, rows)
         view = alls[m].at[p, owner, :]
-        return remote(view, view, cs_sem.at[m, p, k], cr_sem.at[m, p, k], mate)
+        return remote(view, view, cs_sem.at[m, k], cr_sem.at[m, p, k], mate)
 
     def spread_out(p, m):
         for k in range(1, wide):
             to_wide(p, m, k).start()
         to_mate(p, m, 0).start()
 
-    def attend(p):
+    def attend(p, between):
         project(p, order[-1])
         slot = lax.rem(p, 2)
         offset = key_row - jnp.where(query_row < SEG, 0, SEG)
@@ -332,6 +332,8 @@
                 def _():
                     grad_halo(p).start()
 
+                between()
+
         flip_row = lax.broadcasted_iota(jnp.int32, (KB, KB), 0)
         flip_col = lax.broadcasted_iota(jnp.int32, (KB, KB), 1)
         flip = jnp.where(flip_row + flip_col == KB - 1, 1.0, 0.0)
@@ -361,11 +363,11 @@
 
     def to_right(p, m, b):
         view = rights[m].at[p, b]
-        return remote(view, view, rs_sem.at[m, p, b], rv_sem.at[m, p, b], at(z + 1, y, core))
+        return remote(view, view, rs_sem.at[m], rv_sem.at[m, p, b - 1], at(z + 1, y, core))
 
     def to_left(p, m, b):
         view = lefts[m].at[p, b]
-        return remote(view, view, ls_sem.at[m, p, b], lv_sem.at[m, p, b], at(z - 1, y, core))
+        return remote(view, view, ls_sem.at[m], lv_sem.at[m, p, b], at(z - 1, y, core))
 
     def hop(p, m, h):
         @pl.when(z == h)
@@ -482,9 +484,47 @@
         def _():
             gi_ref[:, aligned(j - away, TILE)] = low
 
+    def bias_end():
+        some = far.at[: deep - 1]
+        pltpu.make_async_copy(some, some, br_sem.at[1]).wait()
+        summed = far[0]
+        for n in range(1, deep):
+            summed = summed + far[n]
+        spot = lax.broadcasted_iota(jnp.int32, (rel_ref.shape[1], LINE), 1)
+        back = bias_index(spot - (KB - 1))
+        entry = lax.broadcasted_iota(jnp.int32, (rel_ref.shape[1], LINE), 0)
+        gb_ref[...] = exact(summed, jnp.where(back == entry, 1.0, 0.0), ((1,), (1,)))
+        pltpu.make_async_copy(gb_ref, gb_out, o_sem.at[2]).start()
+
+    def inputs_end():
+        pltpu.make_async_copy(pxr, pxr, pr_sem).wait()
+        for n in range(tiles):
+            cols = slice(n * TILE, (n + 1) * TILE)
+            total = gi_ref[:, cols].astype(F32)
+            for k in range(1, tps):
+                total = total + pxr[(k - 1) * tiles + n].astype(F32)
+            gi_ref[:, cols] = total.astype(BF)
+            pltpu.make_async_copy(gi_ref.at[:, cols], gi_out.at[:, cols], o_sem.at[1]).start()
+
+    def first_sends():
+        for r in order:
+            for k in range(1, tps):
+                x_copy(k, r).wait_send()
+        some = xg.at[: zparts * feat, : (group - 1) * rows]
+        pltpu.make_async_copy(some, some, gs_sem.at[0]).wait()
+        some = xg.at[: (deep - zparts) * feat, : (group - 1) * HALO]
+        pltpu.make_async_copy(some, some, gs_sem.at[1]).wait()
+        some = xg.at[: (deep - zparts) * feat, : (group - 1) * (rows - HALO)]
+        pltpu.make_async_copy(some, some, gs_sem.at[2]).wait()
+
+        @pl.when(has_ahead)
+        def _():
+            halo_copy(k_ext, 0).wait_send()
+            halo_copy(v_ext, 1).wait_send()
+
     hops = deep - 2
     early_pieces = pairs - 1
-    last = 3 + 2 * (hops + 1)
+    last = 5 + hops
     rounds = 2 * pairs + last
     per = 2
 
@@ -511,13 +551,16 @@
 
     @pl.loop(0, rounds)
     def _(i):
-        staged(i, 0, attend)
+        staged(i, 0, functools.partial(attend, between=lambda: pieced(i, 3, product)))
 
         @pl.when(i == pairs - 1)
         def _():
             bias_near()
 
-        staged(i, 1, settle)
+        for lag in (1, 2):
+            @pl.when((i < pairs) if lag == 1 else (i == pairs + 1))
+            def _():
+                staged(i, lag, settle)
         for m in range(2):
             @pl.when((i < early_pieces) & (lax.rem(i, 2) == m))
             def _():
@@ -530,97 +573,80 @@
                 turn(mod(tp - k, tps), r, k - 1)
                 share(mod(tp - k, tps), r * CHUNK, (r + 1) * CHUNK, 1, afar=False)
 
-        @pl.when(i == pairs)
-        def _():
-            for m in (1, 0):
-                for p in range(pairs):
-                    if 2 * p + m >= early_pieces:
-                        spread_out(p, m)
-
-        pieced(i, 3, product)
+        @pl.when(i == pairs - 1)
+        def _():
+            for p in range(early_pieces // 2, pairs - 1):
+                spread_out(p, 1)
+
+        @pl.when(i == pairs + 1)
+        def _():
+            spread_out(pairs - 1, 1)
+            for p in range((early_pieces + 1) // 2, pairs):
+                spread_out(p, 0)
+
+        @pl.when(i >= pairs)
+        def _():
+            pieced(i, 3, product)
+
         for h in range(1, hops + 1):
-            pieced(i, 3 + 2 * h, functools.partial(hop, h=h))
+            pieced(i, 3 + h, functools.partial(hop, h=h))
         pieced(i, last, finish)
         pieced(i, 2, forward)
 
+        @pl.when(i == pairs + 2)
+        def _():
+            first_sends()
+
+        @pl.when(i == rounds - 3)
+        def _():
+            inputs_end()
+
+        @pl.when(i == rounds - 2)
+        def _():
+            bias_end()
+
         @pl.when(i == pairs + 3)
         def _():
             bias_far()
 
-        @pl.when(i >= pairs)
+        @pl.when(i > pairs)
         def _():
             @pl.loop(0, per)
             def _(n):
-                j = (i - pairs) * per + n
+                j = (i - pairs - 1) * per + n
 
                 @pl.when(j < tps * tiles)
                 def _():
                     input_tile(j)
 
-    some = far.at[: deep - 1]
-    pltpu.make_async_copy(some, some, br_sem.at[1]).wait()
-    summed = far[0]
-    for n in range(1, deep):
-        summed = summed + far[n]
-    spot = lax.broadcasted_iota(jnp.int32, (rel_ref.shape[1], LINE), 1)
-    back = bias_index(spot - (KB - 1))
-    entry = lax.broadcasted_iota(jnp.int32, (rel_ref.shape[1], LINE), 0)
-    gb_ref[...] = exact(summed, jnp.where(back == entry, 1.0, 0.0), ((1,), (1,)))
-
-    pltpu.make_async_copy(gb_ref, gb_out, o_sem.at[2]).start()
-    pltpu.make_async_copy(pxr, pxr, pr_sem).wait()
-    for n in range(tiles):
-        cols = slice(n * TILE, (n + 1) * TILE)
-        total = gi_ref[:, cols].astype(F32)
-        for k in range(1, tps):
-            total = total + pxr[(k - 1) * tiles + n].astype(F32)
-        gi_ref[:, cols] = total.astype(BF)
-        pltpu.make_async_copy(gi_ref.at[:, cols], gi_out.at[:, cols], o_sem.at[1]).start()
-
     pltpu.make_async_copy(pxs, pxs, ps_sem).wait()
-    for r in order:
-        for k in range(1, tps):
-            x_copy(k, r).wait_send()
-    some = xg.at[: zparts * feat, : (group - 1) * rows]
-    pltpu.make_async_copy(some, some, gs_sem.at[0]).wait()
-    some = xg.at[: (deep - zparts) * feat, : (group - 1) * HALO]
-    pltpu.make_async_copy(some, some, gs_sem.at[1]).wait()
-    some = xg.at[: (deep - zparts) * feat, : (group - 1) * (rows - HALO)]
-    pltpu.make_async_copy(some, some, gs_sem.at[2]).wait()
-
-    @pl.when(has_ahead)
+    for m in range(2):
+        for zi in range(deep):
+            @pl.when(z == zi)
+            def _():
+                if zi < deep - 1:
+                    some = rights[m].at[:, : deep - 1 - zi]
+                    pltpu.make_async_copy(some, some, rs_sem.at[m]).wait()
+                if zi:
+                    some = lefts[m].at[:, :zi]
+                    pltpu.make_async_copy(some, some, ls_sem.at[m]).wait()
+        some = alls[m].at[:, :rows]
+        for k in range(1, wide):
+            pltpu.make_async_copy(some, some, ys_sem.at[m, k - 1]).wait()
+        for k in range(wide):
+            pltpu.make_async_copy(some, some, cs_sem.at[m, k]).wait()
+
+    @pl.when(has_behind)
     def _():
-        halo_copy(k_ext, 0).wait_send()
-        halo_copy(v_ext, 1).wait_send()
+        pltpu.make_async_copy(halo_s, halo_s, hs_sem).wait()
 
     for j, i in mates:
         near_copy(j, i).wait_send()
     for k in range(1, deep):
         far_copy(k).wait_send()
-
-    @pl.loop(0, pairs)
-    def _(p):
-        @pl.when(has_behind)
-        def _():
-            grad_halo(p).wait_send()
-
-        for m in range(2):
-            for k in range(1, wide):
-                to_wide(p, m, k).wait_send()
-            for k in range(wide):
-                to_mate(p, m, k).wait_send()
-            for b in range(deep):
-                @pl.when(z < b)
-                def _():
-                    to_right(p, m, b).wait_send()
-
-                @pl.when(z > b)
-                def _():
-                    to_left(p, m, b).wait_send()
-
-    pltpu.make_async_copy(dw_ref, dw_out, o_sem.at[0]).wait()
     pltpu.make_async_copy(gi_ref, gi_out, o_sem.at[1]).wait()
     pltpu.make_async_copy(gb_ref, gb_out, o_sem.at[2]).wait()
+    pltpu.make_async_copy(dw_ref, dw_out, o_sem.at[0]).wait()
 
 
 def hand_body(gi, dw, gb, gi_out, dwq_out, dwk_out, dwv_out, gb_out, gi_v, dw_v, gb_v, i_sem, o_sem):
@@ -702,11 +728,11 @@
             dma((tps - 1, chunks)), dma((tps - 1, chunks)),
             dma((3,)), dma((3,)), dma((2,)),
             dma((2,)), dma((2,)),
-            dma((pairs,)), dma((pairs,)),
-            dma((2, pairs, wide - 1)), dma((2, pairs, wide - 1)),
-            dma((2, pairs, wide)), dma((2, pairs, wide)),
-            dma((2, pairs, deep)), dma((2, pairs, deep)),
-            dma((2, pairs, deep)), dma((2, pairs, deep)),
+            dma(()), dma((pairs,)),
+            dma((2, wide - 1)), dma((2, pairs, wide - 1)),
+            dma((2, wide)), dma((2, pairs, wide)),
+            dma((2,)), dma((2, pairs, deep - 1)),
+            dma((2,)), dma((2, pairs, deep - 1)),
             dma((2,)), dma((2,)),
             dma(()), dma(()),
         ],

time: 140 us -> 136 us (0.971)
  Pallas kernels: 139 us -> 135 us
    pallas_call x1, Pallas kernels: 136 us -> 132 us  [local(): pl.pallas_call(functools.partial(step_body, sizes), in_specs=[hbm, hbm, h...]
where the time goes in v4:
time: 136 us
  Pallas kernels  135 us (99%)
    pallas_call x1, Pallas kernels, local(): pl.pallas_call(functools.partial(step_body, sizes), in_specs=[hbm, hbm, h...  132 us
    pallas_call x1, Pallas kernels, local(): pl.pallas_call(hand_body, in_specs=[hbm] * 3, out_specs=[hbm] * 5, out_sh...  2.96 us

profile of v4, /device:TPU:0, one launch (start us, length us, event | category | flops | bytes accessed | tf_op | source)
XLA Modules:
  0.0 135.9 jit_solution(14842752365045434919)
XLA Ops:
  0.6 132.2 %whole_step.1 = (bf16[512,1536]{1,0:T(8,128)(2,1)}, f32[3,192,768]{2,1,0:T(8,128)}, f32[12,320]{1,0:T(8,128)}) custom-call(bf16[512,1536]{1,0:T(8,128)(2,1)} %x_ref.1, bf16[3072,768]{1,0:T(8,128)(2,1)} %wq_ref.1, bf16[3072,768]{1,0:T(8,128)(2,1)} %wk_ref.1, bf16[3072,768]{1,0:T(8,128)(2,1)} %wv_ref.1, f32[12,320]{1,0:T(8,128)} %bitcast.2, bf16[512,768]{1,0:T(8,128)(2,1)} %d_ref.1), custom_call_target="tpu_custom_call" | custom-call | tf_op jit(solution)/shard_map/whole_step/pallas_call | solution.py:685
  132.9 3.0 %hand_out.1 = (bf16[512,1536]{1,0:T(8,128)(2,1)}, f32[192,768]{1,0:T(8,128)}, f32[192,768]{1,0:T(8,128)}, f32[192,768]{1,0:T(8,128)}, f32[12,320]{1,0:T(8,128)}) custom-call(bf16[512,1536]{1,0:T(8,128)(2,1)} %get-tuple-element.13.gi, f32[3,192,768]{2,1,0:T(8,128)} %get-tuple-element.14.dw, f32[12,320]{1,0:T(8,128)} %get-tuple-element.15.gb), custom_call_target="tpu_custom_call" | custom-call | tf_op jit(solution)/shard_map/hand_out/pallas_call | solution.py:745

commit v5 on v4

--- a/solution.py
+++ b/solution.py
@@ -523,7 +523,7 @@
             halo_copy(v_ext, 1).wait_send()
 
     hops = deep - 2
-    early_pieces = pairs - 1
+    early_pieces = max(pairs - 2, 1)
     last = 5 + hops
     rounds = 2 * pairs + last
     per = 2

time: 136 us -> 134 us (0.985)
    pallas_call x1, Pallas kernels: 132 us -> 131 us  [local(): pl.pallas_call(functools.partial(step_body, sizes), in_specs=[hbm, hbm, h...]
where the time goes in v5:
time: 134 us
  Pallas kernels  134 us (100%)
    pallas_call x1, Pallas kernels, local(): pl.pallas_call(functools.partial(step_body, sizes), in_specs=[hbm, hbm, h...  131 us
    pallas_call x1, Pallas kernels, local(): pl.pallas_call(hand_body, in_specs=[hbm] * 3, out_specs=[hbm] * 5, out_sh...  2.96 us

profile of v5, /device:TPU:0, one launch (start us, length us, event | category | flops | bytes accessed | tf_op | source)
XLA Modules:
  0.0 134.2 jit_solution(1260730389018135360)
XLA Ops:
  0.6 130.6 %whole_step.1 = (bf16[512,1536]{1,0:T(8,128)(2,1)}, f32[3,192,768]{2,1,0:T(8,128)}, f32[12,320]{1,0:T(8,128)}) custom-call(bf16[512,1536]{1,0:T(8,128)(2,1)} %x_ref.1, bf16[3072,768]{1,0:T(8,128)(2,1)} %wq_ref.1, bf16[3072,768]{1,0:T(8,128)(2,1)} %wk_ref.1, bf16[3072,768]{1,0:T(8,128)(2,1)} %wv_ref.1, f32[12,320]{1,0:T(8,128)} %bitcast.2, bf16[512,768]{1,0:T(8,128)(2,1)} %d_ref.1), custom_call_target="tpu_custom_call" | custom-call | tf_op jit(solution)/shard_map/whole_step/pallas_call | solution.py:685
  131.2 3.0 %hand_out.1 = (bf16[512,1536]{1,0:T(8,128)(2,1)}, f32[192,768]{1,0:T(8,128)}, f32[192,768]{1,0:T(8,128)}, f32[192,768]{1,0:T(8,128)}, f32[12,320]{1,0:T(8,128)}) custom-call(bf16[512,1536]{1,0:T(8,128)(2,1)} %get-tuple-element.13.gi, f32[3,192,768]{2,1,0:T(8,128)} %get-tuple-element.14.dw, f32[12,320]{1,0:T(8,128)} %get-tuple-element.15.gb), custom_call_target="tpu_custom_call" | custom-call | tf_op jit(solution)/shard_map/hand_out/pallas_call | solution.py:745
